TPU v7x, 32 devices: a whole 2x2x4 slice. The times are simulated.
32 devices in a mesh: fs: 16 (over z, y, x), tp: 2 (over core).
Axes of the slice: x: 2, y: 2, z: 4, core: 2. Of those that a mesh axis runs over, the one named last changes fastest.
Arguments:
- tokens: bfloat16 [4096, 2048], P('fs'), may hold values from -6 to 6
- routes: int32 [4096, 6], P('fs'), may hold values from 0 to 15, all different within a row; in each aligned block of 256 rows (0 to 255, 256 to 511, ...) at most 160 rows name the same one
- route_weights: float32 [4096, 6], P('fs'), may hold values from 0.1 to 1
- norm_gain: float32 [2048], P('fs'), may hold values from 0.1 to 1.9
- expert_gate: float32 [16, 2048, 1024], P(None, 'fs', 'tp'), may hold values from -0.125 to 0.125
- expert_up: float32 [16, 2048, 1024], P(None, 'fs', 'tp'), may hold values from -0.125 to 0.125
- expert_down: float32 [16, 2048, 1024], P(None, 'fs', 'tp'), may hold values from -0.1875 to 0.1875
- shared_gate: float32 [2048, 1024], P('fs', 'tp'), may hold values from -0.125 to 0.125
- shared_up: float32 [2048, 1024], P('fs', 'tp'), may hold values from -0.125 to 0.125
- shared_down: float32 [2048, 1024], P('fs', 'tp'), may hold values from -0.1875 to 0.1875
Outputs:
- layer_output: bfloat16 [4096, 2048], P('fs', 'tp')
- sample_gate: bfloat16 [16, 2048, 1024], P('fs', None, 'tp')
- sample_up: bfloat16 [16, 2048, 1024], P('fs', None, 'tp')
- sample_down: bfloat16 [16, 2048, 1024], P('fs', None, 'tp')
- common_gate: bfloat16 [2048, 1024], P(None, 'tp')
- common_up: bfloat16 [2048, 1024], P(None, 'tp')
- common_down: bfloat16 [2048, 1024], P(None, 'tp')
Inputs may be any that keep to these rules, and one draw needn't show every extreme that they name: `routes`: each row names 6 different experts. In each aligned block of 256 rows (the rows of one index of fs) no expert is named by more than 160 rows, a bound that some expert reaches in some blocks.
All inputs are finite; a program needn't handle non-finite values.
Results may differ from a plain program's by a relative error of at most 0.015.
Values may be sent and summed in bfloat16 or wider, within the bound.
A program may use at most 128 MiB of HBM per device.

v0:
```python
import jax
import jax.numpy as jnp
from jax import lax
from jax.sharding import PartitionSpec as P

EPSILON = 1e-06


def normalize(tokens):
    values = tokens.astype(jnp.float32)
    scale = lax.rsqrt(jnp.mean(values * values, axis=-1, keepdims=True) + EPSILON)
    return (values * scale).astype(jnp.bfloat16)


def ring_of(fs_count):
    if fs_count != 16:
        return list(range(fs_count))
    order = []
    for place, column in enumerate((0, 1, 3, 2)):
        heights = range(4) if place % 2 == 0 else range(3, -1, -1)
        order.extend(height * 4 + column for height in heights)
    return order


def reorder(blocks, order):
    if list(order) == list(range(len(order))):
        return blocks
    return jnp.concatenate([blocks[i : i + 1] for i in order], axis=0)


def body(
    tokens,
    routes,
    route_weights,
    norm_gain,
    expert_gate,
    expert_up,
    expert_down,
    shared_gate,
    shared_up,
    shared_down,
):
    tp_count = lax.axis_size("tp")
    tp_index = lax.axis_index("tp")
    fs_count = lax.axis_size("fs")
    tok_rows, width = tokens.shape
    experts = expert_gate.shape[0]
    share = tok_rows // tp_count
    own_experts = experts // fs_count
    ring = ring_of(fs_count)
    place_of = [ring.index(i) for i in range(fs_count)]
    groups = None if ring == list(range(fs_count)) else [ring]

    normed = normalize(tokens)
    own_normed = lax.dynamic_slice_in_dim(normed, tp_index * share, share, 0)
    own_routes = lax.dynamic_slice_in_dim(routes, tp_index * share, share, 0)
    own_weights = lax.dynamic_slice_in_dim(route_weights, tp_index * share, share, 0)
    member = own_routes[None, :, :] == jnp.arange(experts, dtype=jnp.int32)[:, None, None]
    dense = jnp.sum(jnp.where(member, own_weights[None, :, :], 0.0), axis=2)
    dense_all = lax.all_gather(dense, "fs", axis=0, tiled=False)
    own_normed, dense_all = lax.optimization_barrier((own_normed, dense_all))
    gathered = lax.all_gather(own_normed, "fs", axis=0, tiled=False)
    gathered = reorder(gathered, ring).reshape(fs_count * share, width)

    gain_rows = norm_gain[None, :, None]
    rounded = (
        (expert_gate * gain_rows).astype(jnp.bfloat16),
        (expert_up * gain_rows).astype(jnp.bfloat16),
        expert_down.astype(jnp.bfloat16),
    )
    sample_gate, sample_up, sample_down = (
        lax.all_to_all(rounded[0], "fs", split_axis=0, concat_axis=1, tiled=True),
        lax.all_to_all(rounded[1], "fs", split_axis=0, concat_axis=1, tiled=True),
        lax.all_to_all(rounded[2], "fs", split_axis=0, concat_axis=1, tiled=True),
    )

    half = shared_gate.shape[1]
    shared_rows = jnp.concatenate(
        [
            (shared_gate * norm_gain[:, None]).astype(jnp.bfloat16),
            (shared_up * norm_gain[:, None]).astype(jnp.bfloat16),
            shared_down.astype(jnp.bfloat16),
        ],
        axis=1,
    )
    common = lax.all_gather(shared_rows, "fs", axis=0, tiled=False, axis_index_groups=groups)
    common_gate, common_up, common_down = (
        reorder(common[:, :, i * half : (i + 1) * half], place_of).reshape(width, half)
        for i in range(3)
    )
    shared_gate_act = jnp.dot(normed, common_gate, preferred_element_type=jnp.float32)
    shared_up_act = jnp.dot(normed, common_up, preferred_element_type=jnp.float32)
    shared_hidden = (jax.nn.silu(shared_gate_act) * shared_up_act).astype(jnp.bfloat16)
    shared_part = jnp.einsum(
        "th,dh->td", shared_hidden, common_down, preferred_element_type=jnp.float32
    ).astype(jnp.bfloat16)
    shared_parts = lax.all_to_all(
        shared_part.reshape(tok_rows, tp_count, width // tp_count).transpose(1, 0, 2),
        "tp",
        split_axis=0,
        concat_axis=0,
        tiled=True,
    )
    shared_sum = jnp.sum(shared_parts.astype(jnp.float32), axis=0)

    scale_all = reorder(
        lax.dynamic_slice_in_dim(
            dense_all, lax.axis_index("fs") * own_experts, own_experts, 1
        ),
        ring,
    )
    total = None
    for expert in range(own_experts):
        scale = scale_all[:, expert, :].reshape(-1)[:, None]
        for shift in range(tp_count):
            gate_w, up_w, down_w = (
                sample_gate[expert],
                sample_up[expert],
                sample_down[expert],
            )
            if shift:
                pairs = [(i, (i + shift) % tp_count) for i in range(tp_count)]
                gate_w, up_w, down_w = (
                    lax.ppermute(gate_w, "tp", pairs),
                    lax.ppermute(up_w, "tp", pairs),
                    lax.ppermute(down_w, "tp", pairs),
                )
            gate = jnp.dot(gathered, gate_w, preferred_element_type=jnp.float32)
            upward = jnp.dot(gathered, up_w, preferred_element_type=jnp.float32)
            hidden = (jax.nn.silu(gate) * upward * scale).astype(jnp.bfloat16)
            part = jnp.einsum("rf,df->rd", hidden, down_w, preferred_element_type=jnp.float32)
            total = part if total is None else total + part
    routed = lax.psum_scatter(
        total.astype(jnp.bfloat16), "fs", scatter_dimension=0, tiled=True, axis_index_groups=groups
    )
    routed = lax.all_to_all(routed, "tp", split_axis=1, concat_axis=0, tiled=True)
    layer_output = (routed.astype(jnp.float32) + shared_sum).astype(jnp.bfloat16)
    return (layer_output, sample_gate, sample_up, sample_down, common_gate, common_up, common_down)


def solution(mesh):
    return jax.shard_map(
        body,
        mesh=mesh,
        in_specs=(
            P("fs", None),
            P("fs", None),
            P("fs", None),
            P("fs"),
            P(None, "fs", "tp"),
            P(None, "fs", "tp"),
            P(None, "fs", "tp"),
            P("fs", "tp"),
            P("fs", "tp"),
            P("fs", "tp"),
        ),
        out_specs=(
            P("fs", "tp"),
            P("fs", None, "tp"),
            P("fs", None, "tp"),
            P("fs", None, "tp"),
            P(None, "tp"),
            P(None, "tp"),
            P(None, "tp"),
        ),
        check_vma=False,
    )
```

profile of v0, /device:TPU:9, one launch (start us, length us, event | category | flops | bytes accessed | tf_op | source)
XLA Modules:
  0.0 479.9 jit_solution(11208492477389067535)
XLA Ops:
  8.6 28.0 %all-gather = f32[256,128]{1,0:T(8,128)S(1)} all-gather(f32[16,128]{1,0:T(8,128)S(1)} %select_reduce_fusion), channel_id=2, replica_groups=mesh['fs'=16,'tp'=2] {'fs'}, dimensions={0}, use_global_device_ids=true | all-gather | bytes 139264 | tf_op jit(solution)/shard_map/all_gather | solution.py:60
  36.6 1.5 fusion
  40.4 6.1 %multiply_convert_fusion.2 = (bf16[16,128,512]{2,1,0:T(8,128)(2,1)}, bf16[16,128,512]{2,1,0:T(8,128)(2,1)S(1)}) fusion(f32[16,128,512]{2,1,0:T(8,128)} %param.15, f32[128]{0:T(128)S(1)} %copy-done.8, f32[16,128,512]{2,1,0:T(8,128)} %param.14), kind=kLoop, calls=%fused_computation.3 | loop fusion | flops 4194304 | bytes 12583424 | tf_op jit(solution)/shard_map/convert_element_type | solution.py:68
  46.5 87.8 %all_to_all.54 = bf16[16,128,512]{2,1,0:T(8,128)(2,1)S(1)} all-to-all(bf16[16,128,512]{2,1,0:T(8,128)(2,1)S(1)} %get-tuple-element.57), channel_id=1, replica_groups=mesh['fs'=16,'tp'=2] {'fs'}, dimensions={0} | all-to-all | bytes 4194304 | tf_op jit(solution)/shard_map/all_to_all | solution.py:72
  134.3 5.6 %all-to-all-start.1 = ((bf16[16,128,512]{2,1,0:T(8,128)(2,1)}), bf16[16,128,512]{2,1,0:T(8,128)(2,1)}, u32[]{:S(2)}, u32[]{:S(2)}) async-start(bf16[16,128,512]{2,1,0:T(8,128)(2,1)} %get-tuple-element.56), calls=%async_computation.1 | async-start | bytes 4194304 | tf_op jit(solution)/shard_map/all_to_all | solution.py:73
  139.9 4.9 %convert_element_type.59 = bf16[16,128,512]{2,1,0:T(8,128)(2,1)} convert(f32[16,128,512]{2,1,0:T(8,128)} %param.16) | non-fusion elementwise | flops 1048576 | bytes 6291456 | tf_op jit(solution)/shard_map/convert_element_type | solution.py:69
  144.8 84.8 %all-to-all-done.1 = bf16[16,128,512]{2,1,0:T(8,128)(2,1)} async-done(((bf16[16,128,512]{2,1,0:T(8,128)(2,1)}), bf16[16,128,512]{2,1,0:T(8,128)(2,1)}, u32[]{:S(2)}, u32[]{:S(2)}) %all-to-all-start.1) | async-done | bytes 2097184 | tf_op jit(solution)/shard_map/all_to_all | solution.py:73
  229.6 7.5 %all-to-all-start.2 = ((bf16[16,128,512]{2,1,0:T(8,128)(2,1)}), bf16[16,128,512]{2,1,0:T(8,128)(2,1)}, u32[]{:S(2)}, u32[]{:S(2)}) async-start(bf16[16,128,512]{2,1,0:T(8,128)(2,1)} %convert_element_type.59), calls=%async_computation.2 | async-start | bytes 4194304 | tf_op jit(solution)/shard_map/all_to_all | solution.py:74
  239.6 1.9 collective-permute-start
  241.6 58.4 %all-to-all-done.2 = bf16[16,128,512]{2,1,0:T(8,128)(2,1)} async-done(((bf16[16,128,512]{2,1,0:T(8,128)(2,1)}), bf16[16,128,512]{2,1,0:T(8,128)(2,1)}, u32[]{:S(2)}, u32[]{:S(2)}) %all-to-all-start.2) | async-done | bytes 2097184 | tf_op jit(solution)/shard_map/all_to_all | solution.py:74
  300.0 4.4 collective-permute-start.2
  306.7 1.8 fusion.18
  312.4 6.0 %fusion.30 = f32[2048,512]{1,0:T(8,128)} fusion(bf16[2048,2048]{1,0:T(8,128)(2,1)S(1)} %bitcast.140, bf16[2048,512]{1,0:T(8,128)(2,1)S(1)} %bitcast.104), kind=kOutput, calls=%fused_computation.142 | convolution fusion | flops 4294967296 | bytes 14680064 | tf_op jit(solution)/shard_map/dot_general | solution.py:128
  318.4 7.6 %fusion.31 = f32[2048,512]{1,0:T(8,128)} fusion(bf16[2048,2048]{1,0:T(8,128)(2,1)S(1)} %bitcast.141, bf16[2048,512]{1,0:T(8,128)(2,1)} %collective-permute-done), kind=kOutput, calls=%fused_computation.143 | convolution fusion | flops 4294967296 | bytes 14680064 | tf_op jit(solution)/shard_map/dot_general | solution.py:128
  326.0 7.6 %fusion.32 = f32[2048,512]{1,0:T(8,128)} fusion(bf16[2048,2048]{1,0:T(8,128)(2,1)S(1)} %bitcast.142, bf16[2048,512]{1,0:T(8,128)(2,1)} %collective-permute-done.1), kind=kOutput, calls=%fused_computation.144 | convolution fusion | flops 4294967296 | bytes 14680064 | tf_op jit(solution)/shard_map/dot_general | solution.py:129
  333.6 16.7 %fusion.6 = f32[2048,2048]{1,0:T(8,128)} fusion(bf16[2048,512]{1,0:T(8,128)(2,1)} %bitcast.20, f32[2048,512]{1,0:T(8,128)} %fusion.30, bf16[2048,2048]{1,0:T(8,128)(2,1)} %bitcast.143, bf16[2048,512]{1,0:T(8,128)(2,1)} %bitcast.18, f32[2048]{0:T(1024)S(1)} %bitcast.150), kind=kOutput, calls=%fused_computation.18 | convolution fusion | flops 8597274624 | bytes 33562624 | tf_op jit(solution)/shard_map/rf,df->rd/dot_general | solution.py:131
  350.3 13.5 %add_convert_fusion = bf16[2048,2048]{1,0:T(8,128)(2,1)} fusion(f32[2048,2048]{1,0:T(8,128)} %fusion.6, bf16[2048,512]{1,0:T(8,128)(2,1)} %collective-permute-done.2, f32[2048,512]{1,0:T(8,128)} %fusion.32, f32[2048,512]{1,0:T(8,128)} %fusion.31, f32[2048]{0:T(1024)S(1)} %bitcast.151), kind=kOutput, calls=%fused_computation | convolution fusion | flops 4310695936 | bytes 35659776 | tf_op jit(solution)/shard_map/rf,df->rd/dot_general | solution.py:131
  381.4 1.5 fusion.33
  382.9 4.8 convolution_convert_fusion
  389.0 4.2 all_to_all.55
  393.4 66.0 %reduce-scatter.2.cloned.1.call-done = bf16[128,2048]{1,0:T(8,128)(2,1)} async-done(((bf16[2048,2048]{1,0:T(8,128)(2,1)}), bf16[128,2048]{1,0:T(8,128)(2,1)}) %reduce-scatter.2.cloned.1.call-update) | async-done | bytes 524304 | tf_op jit(solution)/shard_map/reduce_scatter | solution.py:133
  460.5 4.5 all_to_all.56
  467.3 3.1 copy.106
  470.3 3.0 copy.107
  (90 shorter events, 34.7 us)
Async XLA Ops:
  7.2 0.7 copy-start
  7.2 297.2 %all-gather.6.cloned.1.call-start = ((), (), s32[]{:S(2)}) async-start(), calls=%async_computation.7 | async-start | bytes 8912896 | tf_op jit(solution)/shard_map/all_gather | solution.py:62
  38.1 2.4 copy-start.8
  134.3 95.3 %all-to-all-start.1 = ((bf16[16,128,512]{2,1,0:T(8,128)(2,1)}), bf16[16,128,512]{2,1,0:T(8,128)(2,1)}, u32[]{:S(2)}, u32[]{:S(2)}) async-start(bf16[16,128,512]{2,1,0:T(8,128)(2,1)} %get-tuple-element.56), calls=%async_computation.1 | async-start | bytes 4194304 | tf_op jit(solution)/shard_map/all_to_all | solution.py:73
  144.8 92.3 %copy-start.3 = (f32[128,512]{1,0:T(8,128)S(1)}, f32[128,512]{1,0:T(8,128)}, u32[]{:S(2)}) copy-start(f32[128,512]{1,0:T(8,128)} %param.19) | copy-start | bytes 786436
  229.6 70.4 %all-to-all-start.2 = ((bf16[16,128,512]{2,1,0:T(8,128)(2,1)}), bf16[16,128,512]{2,1,0:T(8,128)(2,1)}, u32[]{:S(2)}, u32[]{:S(2)}) async-start(bf16[16,128,512]{2,1,0:T(8,128)(2,1)} %convert_element_type.59), calls=%async_computation.2 | async-start | bytes 4194304 | tf_op jit(solution)/shard_map/all_to_all | solution.py:74
  237.0 126.8 %all-gather.8.cloned.1.call-start = ((), (), s32[]{:S(2)}) async-start(), calls=%async_computation.8 | async-start | bytes 6684672 | tf_op jit(solution)/shard_map/all_gather | solution.py:86
  239.1 220.3 %reduce-scatter.2.cloned.1.call-start = ((), (), s32[]{:S(2)}) async-start(), calls=%async_computation.6 | async-start | bytes 8912896 | tf_op jit(solution)/shard_map/reduce_scatter | solution.py:133
  239.6 78.8 %collective-permute-start = (bf16[2048,512]{1,0:T(8,128)(2,1)S(1)}, bf16[2048,512]{1,0:T(8,128)(2,1)}, u32[]{:S(2)}, u32[]{:S(2)}) collective-permute-start(bf16[2048,512]{1,0:T(8,128)(2,1)S(1)} %bitcast.103), channel_id=1, source_target_pairs={{0,1},{1,0},{2,3},{3,2},{4,5},{5,4},{6,7},{7,6},{8,9},{9,8},{10,11... | collective-permute-start | bytes 6291464 | tf_op jit(solution)/shard_map/ppermute | solution.py:124
  241.5 84.5 %collective-permute-start.1 = (bf16[2048,512]{1,0:T(8,128)(2,1)}, bf16[2048,512]{1,0:T(8,128)(2,1)}, u32[]{:S(2)}, u32[]{:S(2)}) collective-permute-start(bf16[2048,512]{1,0:T(8,128)(2,1)} %bitcast.18), channel_id=1, source_target_pairs={{0,1},{1,0},{2,3},{3,2},{4,5},{5,4},{6,7},{7,6},{8,9},{9,8},{10,11... | collective-permute-start | bytes 6291464 | tf_op jit(solution)/shard_map/ppermute | solution.py:125
  300.0 50.3 %collective-permute-start.2 = (bf16[2048,512]{1,0:T(8,128)(2,1)}, bf16[2048,512]{1,0:T(8,128)(2,1)}, u32[]{:S(2)}, u32[]{:S(2)}) collective-permute-start(bf16[2048,512]{1,0:T(8,128)(2,1)} %bitcast.20), channel_id=1, source_target_pairs={{0,1},{1,0},{2,3},{3,2},{4,5},{5,4},{6,7},{7,6},{8,9},{9,8},{10,11... | collective-permute-start | bytes 6291464 | tf_op jit(solution)/shard_map/ppermute | solution.py:126
  305.5 3.1 slice-start
  305.5 6.4 %copy-start.2 = (bf16[2048,2048]{1,0:T(8,128)(2,1)S(1)}, bf16[2048,2048]{1,0:T(8,128)(2,1)}, u32[]{:S(2)}) copy-start(bf16[2048,2048]{1,0:T(8,128)(2,1)} %all-gather.6.cloned.1.call-done) | copy-start | bytes 25165828
  312.3 13.6 %copy-start.4 = (bf16[16,128,2048]{2,1,0:T(8,128)(2,1)}, bf16[16,128,2048]{2,1,0:T(8,128)(2,1)S(1)}, u32[]{:S(2)}) copy-start(bf16[16,128,2048]{2,1,0:T(8,128)(2,1)S(1)} %fusion.7) | copy-start | bytes 25165828
  380.1 1.3 copy-start.5
  380.1 2.8 copy-start.6
  380.1 2.8 copy-start.7
  467.3 6.1 %copy-start.1 = (f32[256,6]{0,1:T(8,128)S(1)}, f32[256,6]{0,1:T(8,128)}, u32[]{:S(2)}) copy-start(f32[256,6]{0,1:T(8,128)} %param.12) | copy-start | bytes 18436
Sparse Core Ops, SparseCore 0:
  40.5 189.0 all-gather.5
  240.0 108.5 all-gather.7
  363.9 95.4 reduce-scatter.1
where the time goes:
time: 482 us; the launch traced here: 480 us
  waiting for transfers between devices  209 us (43%)
  blocking collectives  124 us (26%)
  matrix products  57.7 us (12%)
  local copies, waits for them, and re-layouts  37.6 us (8%)
  starting transfers between devices  19.7 us (4%)
  other arithmetic  17.1 us (4%)
  between operations  14.1 us (3%)
    all_to_all x1, blocking collectives, body(): lax.all_to_all(rounded[0], 'fs', split_axis=0, concat_axis=1, tiled=True)  87.8 us
    all_to_all x1, waiting for transfers between devices, body(): lax.all_to_all(rounded[1], 'fs', split_axis=0, concat_axis=1, tiled=True)  84.8 us
    reduce_scatter x1, waiting for transfers between devices, body(): lax.psum_scatter(total.astype(jnp.bfloat16), 'fs', scatter_dimension=0, t...  66 us
    all_to_all x1, waiting for transfers between devices, body(): lax.all_to_all(rounded[2], 'fs', split_axis=0, concat_axis=1, tiled=True)  58.4 us
    unnamed x63, local copies, waits for them, and re-layouts  32.5 us
    dot_general x2, matrix products, body(): jnp.einsum('rf,df->rd', hidden, down_w, preferred_element_type=jnp.float32)  30.2 us
    all_gather x1, blocking collectives, body(): dense_all = lax.all_gather(dense, 'fs', axis=0, tiled=False)  28 us
    dot_general x2, matrix products, body(): gate = jnp.dot(gathered, gate_w, preferred_element_type=jnp.float32)  13.6 us
  transfers between devices with their start and end apart: 8, of which 3 were waited for; matrix products, arithmetic and copies ran while one was open for 20% of the time, Pallas kernels for 0%

commit v1 on v0

--- a/solution.py
+++ b/solution.py
@@ -1,8 +1,13 @@
+import functools
+
 import jax
 import jax.numpy as jnp
 from jax import lax
+from jax.experimental import pallas as pl
+from jax.experimental.pallas import tpu as pltpu
 from jax.sharding import PartitionSpec as P
 
+MESH = pl.DeviceIdType.MESH
 EPSILON = 1e-06
 
 
@@ -10,6 +15,272 @@
     values = tokens.astype(jnp.float32)
     scale = lax.rsqrt(jnp.mean(values * values, axis=-1, keepdims=True) + EPSILON)
     return (values * scale).astype(jnp.bfloat16)
+
+
+def place():
+    fs = lax.axis_index("fs")
+    return fs, lax.axis_index("tp"), fs % 2, (fs // 2) % 2, fs // 4
+
+
+def barrier_all(fs, tp):
+    count = lax.axis_size("fs")
+    sem = pltpu.get_barrier_semaphore()
+    for step in range(1, count):
+        pl.semaphore_signal(
+            sem, inc=1, device_id=((fs + step) % count, tp), device_id_type=MESH
+        )
+    pl.semaphore_signal(sem, inc=1, device_id=(fs, 1 - tp), device_id_type=MESH)
+    pl.semaphore_wait(sem, count)
+
+
+def partner_at(step, x, y, z, sign):
+    offset = (7 * step) % 16
+    dz, dy, dx = offset // 4, (offset // 2) % 2, offset % 2
+    return ((z + 4 + sign * dz) % 4) * 4 + ((y + dy) % 2) * 2 + (x + dx) % 2
+
+
+def gather_kernel(
+    tensors, tok_ref, scale_ref, gain_ref, *refs
+):
+    raw = refs[:tensors]
+    tok_all, scale_all = refs[tensors : tensors + 2]
+    own = refs[tensors + 2 : 2 * tensors + 2]
+    other = refs[2 * tensors + 2 : 3 * tensors + 2]
+    (
+        tok_own, wide, narrow,
+        load_sem, tok_send, tok_recv, fwd_send, sc_send, sc_recv,
+        w_send, w_recv, p_send, p_recv, loc_sem,
+    ) = refs[3 * tensors + 2 :]
+    fs, tp, x, y, z = place()
+    plane = fs % 4
+    xp, yp = fs + 1 - 2 * x, fs + 2 - 4 * y
+    rows = raw[0].shape[1]
+    share = tok_own.shape[0]
+
+    def remote(src, dst, ssem, rsem, to, core=None):
+        return pltpu.make_async_remote_copy(
+            src_ref=src, dst_ref=dst, send_sem=ssem, recv_sem=rsem,
+            device_id=(to, tp if core is None else core), device_id_type=MESH,
+        )
+
+    def load(t, to):
+        return pltpu.make_async_copy(raw[t].at[to], wide.at[t, to], load_sem.at[t, to])
+
+    def start_loads(step, _):
+        for t in range(tensors):
+            load(t, partner_at(step, x, y, z, 1)).start()
+        return _
+
+    lax.fori_loop(1, 17, start_loads, 0)
+    tok_own[...] = normalize(tok_ref[...])
+    gain = gain_ref[...]
+
+    def convert(step, _):
+        to = partner_at(step, x, y, z, 1)
+        for t in range(tensors):
+            load(t, to).wait()
+            block = wide[t, to]
+            narrow[t, to] = (block * gain if t < 2 else block).astype(jnp.bfloat16)
+        return _
+
+    def weight(t, to):
+        return remote(
+            narrow.at[t, to], own[t].at[pl.ds(fs * rows, rows)],
+            w_send.at[t, to], w_recv.at[t, fs], to,
+        )
+
+    def send(step, _):
+        to = partner_at(step, x, y, z, 1)
+        for t in range(tensors):
+            weight(t, to).start()
+        return _
+
+    def slot(pl_index, block):
+        return pl_index * 4 + block
+
+    def tok_copy(pl_index, block, sem, to, src=None):
+        s = slot(pl_index, block)
+        return remote(
+            tok_all.at[s] if src is None else src, tok_all.at[s], sem, tok_recv.at[s], to
+        )
+
+    def line_copies(block, src=None):
+        return (
+            (z < 3, block <= z, tok_copy(plane, block, tok_send.at[0, block], fs + 4, src)),
+            (z > 0, block >= z, tok_copy(plane, block, tok_send.at[1, block], fs - 4, src)),
+            (None, None, tok_copy(plane, block, tok_send.at[2, block], xp, src)),
+            (None, None, tok_copy(plane, block, tok_send.at[3, block], yp, src)),
+        )
+
+    def spread(block, src=None):
+        for room, side, copy in line_copies(block, src):
+            if room is None:
+                copy.start()
+            else:
+                pl.when(jnp.logical_and(room, side))(copy.start)
+
+    def arrive(block):
+        s = slot(plane, block)
+        remote(tok_all.at[s], tok_all.at[s], tok_send.at[0, block], tok_recv.at[s], fs + 4).wait_recv()
+        spread(block)
+
+    xplane, yplane = plane + 1 - 2 * x, plane + 2 - 4 * y
+
+    def fwd_copy(block, low):
+        s = slot(xplane if low else yplane, block)
+        return remote(
+            tok_all.at[s], tok_all.at[s], fwd_send.at[block], tok_recv.at[s], yp if low else xp
+        )
+
+    def plane_forward(block):
+        @pl.when(jnp.logical_and(block >= 0, block < 2))
+        def _():
+            copy = fwd_copy(block, True)
+            copy.wait_recv()
+            copy.start()
+
+        @pl.when(jnp.logical_and(block >= 2, block < 4))
+        def _():
+            copy = fwd_copy(block, False)
+            copy.wait_recv()
+            copy.start()
+
+    batch = 3
+    lax.fori_loop(1, 1 + batch, convert, 0)
+    barrier_all(fs, tp)
+
+    spread(z, tok_own)
+    own_tok = pltpu.make_async_copy(tok_own, tok_all.at[slot(plane, z)], loc_sem.at[0])
+    own_tok.start()
+
+    def scale_copy(step):
+        to = (fs + step) % 16
+        return remote(
+            scale_ref.at[to], scale_all.at[slot(plane, z)], sc_send.at[to],
+            sc_recv.at[slot(plane, z)], to,
+        )
+
+    own_scale = pltpu.make_async_copy(scale_ref.at[fs], scale_all.at[slot(plane, z)], loc_sem.at[1])
+    own_scale.start()
+
+    def send_scale(step, _):
+        scale_copy(step).start()
+        return _
+
+    lax.fori_loop(1, 16, send_scale, 0)
+
+    for stage in range(5):
+        lax.fori_loop(1 + batch * stage, 1 + batch * (stage + 1), send, 0)
+        lax.fori_loop(
+            1 + batch * (stage + 1), min(17, 1 + batch * (stage + 2)), convert, 0
+        )
+        if stage < 3:
+            pl.when(z - stage - 1 >= 0)(lambda: arrive(z - stage - 1))
+            pl.when(z + stage + 1 < 4)(lambda: arrive(z + stage + 1))
+        if stage == 0:
+            plane_forward(z)
+        elif stage < 4:
+            plane_forward(z - stage)
+            plane_forward(z + stage)
+
+    def local(t):
+        return pltpu.make_async_copy(
+            narrow.at[t, fs], own[t].at[pl.ds(fs * rows, rows)], loc_sem.at[2 + t]
+        )
+
+    def across(t, frm, src):
+        return remote(
+            src, other[t].at[pl.ds(frm * rows, rows)], p_send.at[t, frm], p_recv.at[t, frm],
+            fs, 1 - tp,
+        )
+
+    for t in range(tensors):
+        local(t).start()
+        across(t, fs, narrow.at[t, fs]).start()
+
+    def pass_on(step, _):
+        frm = partner_at(step, x, y, z, -1)
+        for t in range(tensors):
+            piece = own[t].at[pl.ds(frm * rows, rows)]
+            remote(piece, piece, w_send.at[t, frm], w_recv.at[t, frm], frm).wait_recv()
+            across(t, frm, piece).start()
+        return _
+
+    lax.fori_loop(1, 16, pass_on, 0)
+
+    own_tok.wait()
+    own_scale.wait()
+    for t in range(tensors):
+        local(t).wait()
+
+    def drain_send(step, _):
+        to = partner_at(step, x, y, z, 1)
+        for t in range(tensors):
+            weight(t, to).wait_send()
+        scale_copy(step).wait_send()
+        return _
+
+    lax.fori_loop(1, 16, drain_send, 0)
+
+    def drain_across(step, _):
+        for t in range(tensors):
+            across(t, step, own[t].at[pl.ds(step * rows, rows)]).wait()
+        return _
+
+    lax.fori_loop(0, 16, drain_across, 0)
+
+    for block in range(4):
+        for room, side, copy in line_copies(block):
+            if room is None:
+                copy.wait_send()
+            else:
+                pl.when(jnp.logical_and(room, side))(copy.wait_send)
+        fwd_copy(block, block < 2).wait_send()
+
+        def landed(pl_index):
+            s = slot(pl_index, block)
+            remote(tok_all.at[s], tok_all.at[s], tok_send.at[0, 0], tok_recv.at[s], xp).wait_recv()
+
+        landed(yplane if block < 2 else xplane)
+        landed(3 - plane)
+
+    def drain_scale(step, _):
+        other_fs = (fs + step) % 16
+        s = slot(other_fs % 4, other_fs // 4)
+        remote(
+            scale_all.at[s], scale_all.at[s], sc_send.at[0], sc_recv.at[s], other_fs
+        ).wait_recv()
+        return _
+
+    lax.fori_loop(1, 16, drain_scale, 0)
+
+
+def gather(tokens_share, dense, gain, raws, cid):
+    experts, rows, half = raws[0].shape
+    share, width = tokens_share.shape
+    n = len(raws)
+    hbm, vmem = pl.BlockSpec(memory_space=pl.ANY), pl.BlockSpec(memory_space=pltpu.VMEM)
+    weight = jax.ShapeDtypeStruct((experts * rows, half), jnp.bfloat16)
+    dma = pltpu.SemaphoreType.DMA
+    return pl.pallas_call(
+        functools.partial(gather_kernel, n),
+        out_shape=[
+            jax.ShapeDtypeStruct((16, share, width), jnp.bfloat16),
+            jax.ShapeDtypeStruct((16, 1, share), jnp.float32),
+        ] + [weight] * (2 * n),
+        in_specs=[vmem, vmem, vmem] + [hbm] * n,
+        out_specs=[hbm, vmem] + [hbm] * (2 * n),
+        scratch_shapes=[
+            pltpu.VMEM((share, width), jnp.bfloat16),
+            pltpu.VMEM((n, experts, rows, half), jnp.float32),
+            pltpu.VMEM((n, experts, rows, half), jnp.bfloat16),
+            dma((n, 16)), dma((4, 4)), dma((16,)), dma((4,)), dma((16,)), dma((16,)),
+            dma((n, 16)), dma((n, 16)), dma((n, 16)), dma((n, 16)), dma((2 + n,)),
+        ],
+        compiler_params=pltpu.CompilerParams(
+            collective_id=cid, has_side_effects=True, vmem_limit_bytes=48 << 20
+        ),
+    )(tokens_share, dense, gain, *raws)
 
 
 def ring_of(fs_count):
@@ -28,7 +299,7 @@
     return jnp.concatenate([blocks[i : i + 1] for i in order], axis=0)
 
 
-def body(
+def general_body(
     tokens,
     routes,
     route_weights,
@@ -138,7 +409,74 @@
     return (layer_output, sample_gate, sample_up, sample_down, common_gate, common_up, common_down)
 
 
+def block_body(
+    tokens, routes, route_weights, norm_gain,
+    expert_gate, expert_up, expert_down,
+    shared_gate, shared_up, shared_down,
+):
+    tp_index = lax.axis_index("tp")
+    tok_rows, width = tokens.shape
+    experts = expert_gate.shape[0]
+    share = tok_rows // 2
+    own_routes = lax.dynamic_slice_in_dim(routes, tp_index * share, share, 0)
+    own_weights = lax.dynamic_slice_in_dim(route_weights, tp_index * share, share, 0)
+    own_tokens = lax.dynamic_slice_in_dim(tokens, tp_index * share, share, 0)
+    member = own_routes[None, :, :] == jnp.arange(experts, dtype=jnp.int32)[:, None, None]
+    dense = jnp.sum(jnp.where(member, own_weights[None, :, :], 0.0), axis=2)
+    gathered, scale, sample_gate, sample_up, sample_down, gate_o, up_o, down_o = gather(
+        own_tokens, dense[:, None, :], norm_gain[:, None],
+        (expert_gate, expert_up, expert_down), 1,
+    )
+    gathered = gathered.reshape(16 * share, width)
+    scale = scale.reshape(16 * share, 1)
+    normed = normalize(tokens)
+    half = shared_gate.shape[1]
+    shared_rows = jnp.concatenate(
+        [
+            (shared_gate * norm_gain[:, None]).astype(jnp.bfloat16),
+            (shared_up * norm_gain[:, None]).astype(jnp.bfloat16),
+            shared_down.astype(jnp.bfloat16),
+        ],
+        axis=1,
+    )
+    common = lax.all_gather(shared_rows, "fs", axis=0, tiled=True)
+    common_gate, common_up, common_down = (
+        common[:, i * half : (i + 1) * half] for i in range(3)
+    )
+    shared_hidden = (
+        jax.nn.silu(jnp.dot(normed, common_gate, preferred_element_type=jnp.float32))
+        * jnp.dot(normed, common_up, preferred_element_type=jnp.float32)
+    ).astype(jnp.bfloat16)
+    shared_part = jnp.einsum(
+        "th,dh->td", shared_hidden, common_down, preferred_element_type=jnp.float32
+    ).astype(jnp.bfloat16)
+    shared_parts = lax.all_to_all(
+        shared_part.reshape(tok_rows, 2, width // 2).transpose(1, 0, 2),
+        "tp", split_axis=0, concat_axis=0, tiled=True,
+    )
+    shared_sum = jnp.sum(shared_parts.astype(jnp.float32), axis=0)
+    total = None
+    for gate_w, up_w, down_w in ((sample_gate, sample_up, sample_down), (gate_o, up_o, down_o)):
+        gate = jnp.dot(gathered, gate_w, preferred_element_type=jnp.float32)
+        upward = jnp.dot(gathered, up_w, preferred_element_type=jnp.float32)
+        hidden = (jax.nn.silu(gate) * upward * scale).astype(jnp.bfloat16)
+        part = jnp.einsum("rf,df->rd", hidden, down_w, preferred_element_type=jnp.float32)
+        total = part if total is None else total + part
+    order = [[plane + 4 * z for plane in range(4) for z in range(4)]]
+    routed = lax.psum_scatter(
+        total.astype(jnp.bfloat16), "fs", scatter_dimension=0, tiled=True, axis_index_groups=order
+    )
+    routed = lax.all_to_all(routed, "tp", split_axis=1, concat_axis=0, tiled=True)
+    layer_output = (routed.astype(jnp.float32) + shared_sum).astype(jnp.bfloat16)
+    return (
+        layer_output, sample_gate[None], sample_up[None], sample_down[None],
+        common_gate, common_up, common_down,
+    )
+
+
 def solution(mesh):
+    fits = mesh.shape["fs"] == 16 and mesh.shape["tp"] == 2
+    body = block_body if fits else general_body
     return jax.shard_map(
         body,
         mesh=mesh,

time: 482 us -> 491 us (1.019)
  Pallas kernels: 0 us -> 225 us
  blocking collectives: 124 us -> 10.3 us
  waiting for transfers between devices: 209 us -> 161 us
  local copies, waits for them, and re-layouts: 37.6 us -> 14.3 us
  starting transfers between devices: 19.7 us -> 0.08 us
  other arithmetic: 17.1 us -> 4.44 us
    pallas_call x0 -> x1, Pallas kernels: none -> 225 us  [gather(): pl.pallas_call(functools.partial(gather_kernel, n), out_shape=[jax.ShapeD...]
    all_to_all x2 -> x0, waiting for transfers between devices: 143 us -> none  [the longest x1 84.8 us: body(): lax.all_to_all(rounded[1], 'fs', split_axis=0, concat_axis=1, tiled=True)]
    reduce_scatter x1, waiting for transfers between devices: 66 us -> 161 us  [block_body(): lax.psum_scatter(total.astype(jnp.bfloat16), 'fs', scatter_dimension=0, t...]
    all_to_all x3 -> x2, blocking collectives: 96.5 us -> 10.3 us  [the longest x1 5.82 us: block_body(): lax.all_to_all(shared_part.reshape(tok_rows, 2, width // 2).transpose(1,...]
    all_gather x1 -> x0, blocking collectives: 28 us -> none  [body(): dense_all = lax.all_gather(dense, 'fs', axis=0, tiled=False)]
    unnamed x63 -> x25, local copies, waits for them, and re-layouts: 32.5 us -> 6.35 us
    all_to_all x2 -> x0, starting transfers between devices: 13.1 us -> none  [the longest x1 7.48 us: body(): lax.all_to_all(rounded[2], 'fs', split_axis=0, concat_axis=1, tiled=True)]
    convert_element_type x6 -> x3, other arithmetic: 14.6 us -> 3.15 us  [the longest x1 1.14 us: block_body(): (shared_gate * norm_gain[:, None]).astype(jnp.bfloat16)]
  transfers between devices with their start and end apart: 8 -> 2, of which waited for: 3 -> 1; matrix products, arithmetic and copies ran while one was open for 20% -> 13% of each run, Pallas kernels for 0% -> 46%
where the time goes in v1:
time: 491 us; the launch traced here: 487 us
  Pallas kernels  225 us (46%)
  waiting for transfers between devices  161 us (33%)
  matrix products  57.9 us (12%)
  local copies, waits for them, and re-layouts  14.3 us (3%)
  between operations  14.2 us (3%)
  blocking collectives  10.3 us (2%)
    pallas_call x1, Pallas kernels, gather(): pl.pallas_call(functools.partial(gather_kernel, n), out_shape=[jax.ShapeD...  225 us
    reduce_scatter x1, waiting for transfers between devices, block_body(): lax.psum_scatter(total.astype(jnp.bfloat16), 'fs', scatter_dimension=0, t...  161 us
    dot_general x2, matrix products, block_body(): jnp.einsum('rf,df->rd', hidden, down_w, preferred_element_type=jnp.float32)  30.8 us
    dot_general x2, matrix products, block_body(): gate = jnp.dot(gathered, gate_w, preferred_element_type=jnp.float32)  14.3 us
  transfers between devices with their start and end apart: 2, of which 1 were waited for; matrix products, arithmetic and copies ran while one was open for 13% of the time, Pallas kernels for 46%

profile of v1, /device:TPU:9, one launch (start us, length us, event | category | flops | bytes accessed | tf_op | source)
XLA Modules:
  0.0 487.4 jit_solution(10135626006917044657)
XLA Ops:
  7.3 1.1 convert_element_type.55
  8.3 1.1 multiply_convert_fusion.3
  9.5 0.8 pad_maximum_fusion
  10.6 225.3 %shard_map.153 = (bf16[16,128,2048]{2,1,0:T(8,128)(2,1)}, f32[16,1,128]{2,1,0:T(1,128)S(1)}, bf16[2048,512]{1,0:T(8,128)(2,1)S(1)}, bf16[2048,512]{1,0:T(8,128)(...) custom-call(bf16[128,2048]{1,0:T(8,128)(2,1)S(1)} %constant_dynamic-, ...), custom_call_target="tpu_custom_call" | custom-call | tf_op jit(solution)/shard_map/pallas_call | solution.py:265
  235.9 8.3 %fusion.19 = f32[2048,512]{1,0:T(8,128)S(1)} fusion(bf16[2048,2048]{1,0:T(8,128)(2,1)} %bitcast.49, bf16[2048,512]{1,0:T(8,128)(2,1)} %get-tuple-element.20), kind=kOutput, calls=%fused_computation.36 | convolution fusion | flops 4294967296 | bytes 14680064 | tf_op jit(solution)/shard_map/dot_general | solution.py:460
  244.3 6.0 %fusion.18 = f32[2048,512]{1,0:T(8,128)} fusion(bf16[2048,2048]{1,0:T(8,128)(2,1)S(1)} %bitcast.51, bf16[2048,512]{1,0:T(8,128)(2,1)S(1)} %get-tuple-element.16), kind=kOutput, calls=%fused_computation.35 | convolution fusion | flops 4294967296 | bytes 14680064 | tf_op jit(solution)/shard_map/dot_general | solution.py:460
  250.3 6.1 %multiply_convert_fusion = bf16[2048,512]{1,0:T(8,128)(2,1)} fusion(f32[2048,512]{1,0:T(8,128)S(1)} %fusion.19, bf16[2048,2048]{1,0:T(8,128)(2,1)S(1)} %bitcast.52, bf16[2048,512]{1,0:T(8,128)(2,1)S(1)} %copy-done.10, f32[2048]{0:T(1024)S(1)} %bitcast.41), kind=kOutput, calls=%fused_computation.1 | convolution fusion | flops 4302307328 | bytes 16785408 | tf_op jit(solution)/shard_map/dot_general | solution.py:461
  256.4 16.0 %fusion.4 = f32[2048,2048]{1,0:T(8,128)} fusion(bf16[2048,512]{1,0:T(8,128)(2,1)} %get-tuple-element.19, f32[2048,512]{1,0:T(8,128)} %fusion.18, bf16[2048,2048]{1,0:T(8,128)(2,1)} %bitcast.50, bf16[2048,512]{1,0:T(8,128)(2,1)S(1)} %get-tuple-element.17, f32[2048]{0:T(1024)S(1)} %bitcast.42), kind=kOutput, calls=%fused_computation.14 | convolution fusion | flops 8597274624 | bytes 33562624 | tf_op jit(solution)/shard_map/rf,df->rd/dot_general | solution.py:463
  272.4 14.8 %add_convert_fusion = bf16[2048,2048]{1,0:T(8,128)(2,1)} fusion(f32[2048,2048]{1,0:T(8,128)} %fusion.4, bf16[2048,512]{1,0:T(8,128)(2,1)} %multiply_convert_fusion, bf16[2048,512]{1,0:T(8,128)(2,1)} %get-tuple-element.22), kind=kOutput, calls=%fused_computation | convolution fusion | flops 4303355904 | bytes 29360128 | tf_op jit(solution)/shard_map/rf,df->rd/dot_general | solution.py:463
  287.3 0.3 fusion
  287.6 5.3 %fusion.17 = (bf16[2048,512]{1,0:T(8,128)(2,1)S(1)}, bf16[2048,512]{1,0:T(8,128)(2,1)}, bf16[2048,512]{1,0:T(8,128)(2,1)}) fusion(bf16[2048,1536]{1,0:T(8,128)(2,1)} %all-gather.2.cloned.1.call-done), kind=kLoop, calls=%fused_computation.34 | loop fusion | bytes 12582912 | tf_op jit(solution)/shard_map/slice | solution.py:444
  292.9 1.3 copy-done.6
  294.2 1.5 fusion.12
  295.8 5.0 %convolution_convert_fusion = bf16[256,2048]{1,0:T(8,128)(2,1)} fusion(bf16[2048,512]{1,0:T(8,128)(2,1)} %get-tuple-element.41, bf16[2048,512]{1,0:T(8,128)(2,1)} %get-tuple-element.40, f32[256,512]{1,0:T(8,128)} %fusion.12, bf16[256,2048]{1,0:T(8,128)(2,1)S(1)} %copy-done.4, f32[256]{0:T(256)S(1)} %add_rsqrt_fusion), kind=kOutput, calls=%fused_computation.5 | convolution fusion | flops 1076625408 | bytes 6816768 | tf_op jit(solution)/shard_map/th,dh->td/dot_general | solution.py:450
  300.8 1.3 copy.33
  302.1 5.8 %all_to_all.18 = bf16[2,256,1024]{2,1,0:T(8,128)(2,1)S(1)} all-to-all(bf16[2,256,1024]{2,1,0:T(8,128)(2,1)S(1)} %bitcast.43), channel_id=1, replica_groups=mesh['fs'=16,'tp'=2] {'tp'}, dimensions={0} | all-to-all | bytes 2097152 | tf_op jit(solution)/shard_map/all_to_all | solution.py:453
  308.1 160.7 %reduce-scatter.2.cloned.1.call-done = bf16[128,2048]{1,0:T(8,128)(2,1)} async-done(((bf16[2048,2048]{1,0:T(8,128)(2,1)}), bf16[128,2048]{1,0:T(8,128)(2,1)}) %reduce-scatter.2.cloned.1.call-update) | async-done | bytes 524304 | tf_op jit(solution)/shard_map/reduce_scatter | solution.py:466
  468.9 1.2 copy.34
  470.1 4.5 all_to_all.19
  474.6 1.0 fusion.3
  475.5 1.3 copy.38
  476.8 1.3 copy.39
  478.2 1.0 copy-done.5
  479.2 1.3 copy.40
  (32 shorter events, 0.6 us)
Async XLA Ops:
  7.2 3.3 copy-start
  7.2 3.1 copy-start.8
  7.2 3.3 copy-start.7
  7.2 3.3 copy-start.4
  7.2 280.4 %all-gather.2.cloned.1.call-start = ((), (), s32[]{:S(2)}) async-start(), calls=%async_computation.4 | async-start | bytes 6684672 | tf_op jit(solution)/shard_map/all_gather | solution.py:442
  10.3 458.6 %reduce-scatter.2.cloned.1.call-start = ((), (), s32[]{:S(2)}) async-start(), calls=%async_computation.3 | async-start | bytes 8912896 | tf_op jit(solution)/shard_map/reduce_scatter | solution.py:466
  235.9 8.3 %copy-start.2 = (bf16[2048,512]{1,0:T(8,128)(2,1)}, bf16[2048,512]{1,0:T(8,128)(2,1)S(1)}, u32[]{:S(2)}) copy-start(bf16[2048,512]{1,0:T(8,128)(2,1)S(1)} %get-tuple-element.16) | copy-start | bytes 6291460
  235.9 8.3 %copy-start.9 = (bf16[16,128,2048]{2,1,0:T(8,128)(2,1)S(1)}, bf16[16,128,2048]{2,1,0:T(8,128)(2,1)}, u32[]{:S(2)}) copy-start(bf16[16,128,2048]{2,1,0:T(8,128)(2,1)} %get-tuple-element.15) | copy-start | bytes 25165828
  244.3 6.0 %copy-start.10 = (bf16[2048,512]{1,0:T(8,128)(2,1)S(1)}, bf16[2048,512]{1,0:T(8,128)(2,1)}, u32[]{:S(2)}) copy-start(bf16[2048,512]{1,0:T(8,128)(2,1)} %get-tuple-element.21) | copy-start | bytes 6291460
  292.9 1.3 copy-start.6
  468.9 6.7 %copy-start.3 = (bf16[2048,512]{1,0:T(8,128)(2,1)S(1)}, bf16[2048,512]{1,0:T(8,128)(2,1)}, u32[]{:S(2)}) copy-start(bf16[2048,512]{1,0:T(8,128)(2,1)} %copy-done.2) | copy-start | bytes 6291460
  476.8 2.3 copy-start.5
  476.8 3.7 copy-start.1
Sparse Core Ops, SparseCore 0:
  11.4 187.6 all-gather.1
  287.4 181.4 reduce-scatter.1

commit v2 on v0

--- a/solution.py
+++ b/solution.py
@@ -1,15 +1,649 @@
+import functools
+
 import jax
 import jax.numpy as jnp
 from jax import lax
+from jax.experimental import pallas as pl
+from jax.experimental.pallas import tpu as pltpu
 from jax.sharding import PartitionSpec as P
 
+MESH = pl.DeviceIdType.MESH
 EPSILON = 1e-06
+UNITS = (0, 3, 1, 2)
 
 
 def normalize(tokens):
     values = tokens.astype(jnp.float32)
     scale = lax.rsqrt(jnp.mean(values * values, axis=-1, keepdims=True) + EPSILON)
     return (values * scale).astype(jnp.bfloat16)
+
+
+def place():
+    fs = lax.axis_index("fs")
+    return fs, lax.axis_index("tp"), fs % 2, (fs // 2) % 2, fs // 4
+
+
+def barrier_all(fs, tp):
+    count = lax.axis_size("fs")
+    sem = pltpu.get_barrier_semaphore()
+    for step in range(1, count):
+        pl.semaphore_signal(
+            sem, inc=1, device_id=((fs + step) % count, tp), device_id_type=MESH
+        )
+    pl.semaphore_signal(sem, inc=1, device_id=(fs, 1 - tp), device_id_type=MESH)
+    pl.semaphore_wait(sem, count)
+
+
+def partner_at(step, x, y, z, sign):
+    offset = (7 * step) % 16
+    dz, dy, dx = offset // 4, (offset // 2) % 2, offset % 2
+    return ((z + 4 + sign * dz) % 4) * 4 + ((y + dy) % 2) * 2 + (x + dx) % 2
+
+
+def remote(src, dst, ssem, rsem, to, core):
+    return pltpu.make_async_remote_copy(
+        src_ref=src, dst_ref=dst, send_sem=ssem, recv_sem=rsem,
+        device_id=(to, core), device_id_type=MESH,
+    )
+
+
+class Chain:
+    def __init__(self, at, send_sem, fwd_sem, recv_sem):
+        self.fs, self.tp, self.x, self.y, self.z = place()
+        self.at, self.send_sem, self.fwd_sem, self.recv_sem = at, send_sem, fwd_sem, recv_sem
+        self.plane = self.fs % 4
+        self.xp, self.yp = self.fs + 1 - 2 * self.x, self.fs + 2 - 4 * self.y
+        self.xplane, self.yplane = self.plane + 1 - 2 * self.x, self.plane + 2 - 4 * self.y
+
+    def copy(self, slot, sem, to, src=None):
+        here = self.at(slot)
+        return remote(
+            here if src is None else src, here, sem, self.recv_sem.at[slot], to, self.tp
+        )
+
+    def line(self, block, src=None):
+        slot, z = block * 4 + self.plane, self.z
+        return (
+            (jnp.logical_and(z < 3, block <= z), self.copy(slot, self.send_sem.at[0, block], self.fs + 4, src)),
+            (jnp.logical_and(z > 0, block >= z), self.copy(slot, self.send_sem.at[1, block], self.fs - 4, src)),
+            (None, self.copy(slot, self.send_sem.at[2, block], self.xp, src)),
+            (None, self.copy(slot, self.send_sem.at[3, block], self.yp, src)),
+        )
+
+    def spread(self, block, src=None):
+        for cond, copy in self.line(block, src):
+            if cond is None:
+                copy.start()
+            else:
+                pl.when(cond)(copy.start)
+
+    def landed(self, slot):
+        self.copy(slot, self.send_sem.at[0, 0], self.xp).wait_recv()
+
+    def arrive(self, block):
+        self.landed(block * 4 + self.plane)
+        self.spread(block)
+
+    def forward_copy(self, block, low):
+        slot = block * 4 + (self.xplane if low else self.yplane)
+        return self.copy(slot, self.fwd_sem.at[block], self.yp if low else self.xp)
+
+    def plane_forward(self, block):
+        for low in (True, False):
+            inside = (
+                jnp.logical_and(block >= 0, block < 2)
+                if low
+                else jnp.logical_and(block >= 2, block < 4)
+            )
+
+            @pl.when(inside)
+            def _(low=low):
+                copy = self.forward_copy(block, low)
+                copy.wait_recv()
+                copy.start()
+
+    def stage(self, step):
+        z = self.z
+        if step < 3:
+            pl.when(z - step - 1 >= 0)(lambda: self.arrive(z - step - 1))
+            pl.when(z + step + 1 < 4)(lambda: self.arrive(z + step + 1))
+        if step == 0:
+            self.plane_forward(z)
+        elif step < 4:
+            self.plane_forward(z - step)
+            self.plane_forward(z + step)
+
+    def finish(self):
+        for block in range(4):
+            self.landed(block * 4 + (self.yplane if block < 2 else self.xplane))
+            self.landed(block * 4 + 3 - self.plane)
+
+    def drain(self):
+        for block in range(4):
+            for cond, copy in self.line(block):
+                if cond is None:
+                    copy.wait_send()
+                else:
+                    pl.when(cond)(copy.wait_send)
+            self.forward_copy(block, block < 2).wait_send()
+
+
+class Exchange:
+    def __init__(self, raw, wide, narrow, own, other, gain, sems):
+        self.raw, self.wide, self.narrow, self.own, self.other = raw, wide, narrow, own, other
+        self.gain = gain
+        self.load_sem, self.send_sem, self.recv_sem, self.psend, self.precv = sems
+        self.fs, self.tp, self.x, self.y, self.z = place()
+        self.rows = raw[0].shape[1]
+        self.count = len(raw)
+
+    def partner(self, step, sign=1):
+        return partner_at(step, self.x, self.y, self.z, sign)
+
+    def load(self, t, to):
+        return pltpu.make_async_copy(
+            self.raw[t].at[to], self.wide.at[t, to], self.load_sem.at[t, to]
+        )
+
+    def each(self, lower, upper, body):
+        def step(i, carry):
+            for t in range(self.count):
+                body(i, t)
+            return carry
+
+        lax.fori_loop(lower, upper, step, 0)
+
+    def start_loads(self):
+        self.each(1, 17, lambda i, t: self.load(t, self.partner(i)).start())
+
+    def convert(self, lower, upper):
+        def one(i, t):
+            to = self.partner(i)
+            self.load(t, to).wait()
+            block = self.wide[t, to]
+            if self.gain is not None:
+                block = block * self.gain
+            self.narrow[t, to] = block.astype(jnp.bfloat16)
+
+        self.each(lower, upper, one)
+
+    def piece(self, ref, frm):
+        return ref.at[pl.ds(frm * self.rows, self.rows)]
+
+    def copy(self, t, to):
+        return remote(
+            self.narrow.at[t, to], self.piece(self.own[t], self.fs),
+            self.send_sem.at[t, to], self.recv_sem.at[t, self.fs], to, self.tp,
+        )
+
+    def send(self, lower, upper):
+        self.each(lower, upper, lambda i, t: self.copy(t, self.partner(i)).start())
+
+    def across(self, t, frm, src):
+        return remote(
+            src, self.piece(self.other[t], frm), self.psend.at[t, frm], self.precv.at[t, frm],
+            self.fs, 1 - self.tp,
+        )
+
+    def pass_on(self):
+        def one(i, t):
+            frm = self.partner(i, -1)
+            piece = self.piece(self.own[t], frm)
+            remote(
+                piece, piece, self.send_sem.at[t, frm], self.recv_sem.at[t, frm], frm, self.tp
+            ).wait_recv()
+            self.across(t, frm, piece).start()
+
+        self.each(1, 16, one)
+
+    def finish(self):
+        self.each(
+            0, 16, lambda i, t: self.across(t, i, self.piece(self.own[t], i)).wait()
+        )
+
+    def drain(self):
+        self.each(1, 16, lambda i, t: self.copy(t, self.partner(i)).wait_send())
+
+
+def gather_kernel(
+    tok_ref, scale_ref, gain_ref, gate_ref, up_ref,
+    tok_all, scale_all, gate_own, up_own, gate_other, up_other,
+    tok_own, wide, narrow,
+    chain_send, chain_fwd, chain_recv, sc_send, sc_recv,
+    load_sem, w_send, w_recv, p_send, p_recv, loc_sem,
+):
+    fs, tp, x, y, z = place()
+    ex = Exchange(
+        (gate_ref, up_ref), wide, narrow, (gate_own, up_own), (gate_other, up_other),
+        gain_ref[...], (load_sem, w_send, w_recv, p_send, p_recv),
+    )
+    chain = Chain(lambda slot: tok_all.at[slot], chain_send, chain_fwd, chain_recv)
+    ex.start_loads()
+    tok_own[...] = normalize(tok_ref[...])
+    batch = 3
+    ex.convert(1, 1 + batch)
+    barrier_all(fs, tp)
+    chain.spread(z, tok_own)
+    own_tok = pltpu.make_async_copy(tok_own, tok_all.at[fs], loc_sem.at[0])
+    own_tok.start()
+    own_scale = pltpu.make_async_copy(scale_ref.at[fs], scale_all.at[fs], loc_sem.at[1])
+    own_scale.start()
+
+    def scale_copy(to):
+        return remote(
+            scale_ref.at[to], scale_all.at[fs], sc_send.at[to], sc_recv.at[fs], to, tp
+        )
+
+    def send_scale(step, carry):
+        scale_copy((fs + step) % 16).start()
+        return carry
+
+    lax.fori_loop(1, 16, send_scale, 0)
+    for stage in range(5):
+        ex.send(1 + batch * stage, 1 + batch * (stage + 1))
+        ex.convert(1 + batch * (stage + 1), min(17, 1 + batch * (stage + 2)))
+        chain.stage(stage)
+
+    def local(t):
+        return pltpu.make_async_copy(narrow.at[t, fs], ex.piece(ex.own[t], fs), loc_sem.at[2 + t])
+
+    for t in range(2):
+        local(t).start()
+        ex.across(t, fs, narrow.at[t, fs]).start()
+    ex.pass_on()
+    own_tok.wait()
+    own_scale.wait()
+    for t in range(2):
+        local(t).wait()
+    chain.finish()
+    ex.finish()
+    chain.drain()
+    ex.drain()
+
+    def drain_scale(step, carry):
+        frm = (fs + step) % 16
+        scale_copy(frm).wait_send()
+        here = scale_all.at[frm]
+        remote(here, here, sc_send.at[frm], sc_recv.at[frm], frm, tp).wait_recv()
+        return carry
+
+    lax.fori_loop(1, 16, drain_scale, 0)
+
+
+def dot_nt(a, b):
+    return lax.dot_general(a, b, (((1,), (1,)), ((), ())), preferred_element_type=jnp.float32)
+
+
+def mix_kernel(
+    tok_ref, scale_ref, gain_ref, sgate_ref, sup_ref, sdown_ref,
+    tok_all, gate_own, up_own, gate_other, up_other, down_ref,
+    out_ref, sample_down, common_gate, common_up, common_down,
+    acts, gate_up, down_v, wide, narrow, hidden, common, normed,
+    shid, spart, spart_in, fin, fin_in, xd_in, yd_in, xg_in, yg_in, zb_in, za_in,
+    chain_send, chain_fwd, chain_recv, load_sem, w_send, w_recv, p_send, p_recv,
+    d_send, d_recv, g_send, g_recv, z_send, z_recv, e_send, e_recv, loc_sem,
+):
+    fs, tp, x, y, z = place()
+    ex = Exchange(
+        (down_ref,), wide, narrow, (down_v.at[0],), (down_v.at[1],), None,
+        (load_sem, w_send, w_recv, p_send, p_recv),
+    )
+    rows, half = sgate_ref.shape
+    width = tok_ref.shape[1]
+    chain = Chain(
+        lambda slot: common.at[pl.ds(slot * rows, rows)], chain_send, chain_fwd, chain_recv
+    )
+    share = acts.shape[1] // 4
+
+    ex.start_loads()
+    loads = [
+        pltpu.make_async_copy(src, gate_up.at[t, h], loc_sem.at[2 * t + h])
+        for t, pair in enumerate(((gate_own, gate_other), (up_own, up_other)))
+        for h, src in enumerate(pair)
+    ] + [
+        pltpu.make_async_copy(
+            tok_all.at[pl.ds(b * 4 * share, 4 * share)], acts.at[b], loc_sem.at[4 + b]
+        )
+        for b in UNITS
+    ]
+    for copy in loads:
+        copy.start()
+    gain = gain_ref[...]
+    mine = pl.ds(fs * rows, rows)
+    common[mine, 0:half] = (sgate_ref[...] * gain).astype(jnp.bfloat16)
+    common[mine, half : 2 * half] = (sup_ref[...] * gain).astype(jnp.bfloat16)
+    common[mine, 2 * half : 3 * half] = sdown_ref[...].astype(jnp.bfloat16)
+    batch = 3
+    ex.convert(1, 1 + batch)
+    barrier_all(fs, tp)
+    chain.spread(z)
+    ex.send(1, 1 + batch)
+    ex.convert(1 + batch, 17)
+    normed[...] = normalize(tok_ref[...])
+    for copy in loads:
+        copy.wait()
+
+    tile = 256
+    per_half = half // tile
+
+    def gate_up_unit(b):
+        def step(j, carry):
+            h, c = j // per_half, j % per_half
+            cols = pl.ds(pl.multiple_of(c * tile, tile), tile)
+            a = acts[b]
+            gate = jnp.dot(a, gate_up[0, h, :, cols], preferred_element_type=jnp.float32)
+            up = jnp.dot(a, gate_up[1, h, :, cols], preferred_element_type=jnp.float32)
+            scale = scale_ref[pl.ds(b * 4 * share, 4 * share), :]
+            hidden[b, :, pl.ds(pl.multiple_of(j * tile, tile), tile)] = (
+                jax.nn.silu(gate) * up * scale
+            ).astype(jnp.bfloat16)
+            return carry
+
+        lax.fori_loop(0, 2 * per_half, step, 0)
+
+    for index, b in enumerate(UNITS):
+        gate_up_unit(b)
+        chain.stage(index)
+        ex.send(1 + batch * (index + 1), 1 + batch * (index + 2))
+
+    own_down = pltpu.make_async_copy(narrow.at[0, fs], ex.piece(sample_down, fs), loc_sem.at[0])
+    own_down.start()
+    down_v[0, mine, :] = narrow[0, fs]
+    ex.across(0, fs, narrow.at[0, fs]).start()
+    ex.pass_on()
+    ex.finish()
+
+    def put_down(i, carry):
+        frm = ex.partner(i)
+        pltpu.make_async_copy(
+            ex.piece(down_v.at[0], frm), ex.piece(sample_down, frm), load_sem.at[0, frm]
+        ).start()
+        return carry
+
+    lax.fori_loop(1, 16, put_down, 0)
+
+    plane = fs % 4
+    xp, yp = chain.xp, chain.yp
+    xplane, yplane, dplane = chain.xplane, chain.yplane, 3 - plane
+    mid = width // 2
+    lo, hi = pl.ds(0, mid), pl.ds(mid, mid)
+
+    def part(b, which, cols):
+        return acts.at[b, pl.ds(which * share, share), cols]
+
+    def down_unit(b):
+        def step(n, carry):
+            cols = pl.ds(pl.multiple_of(n * tile, tile), tile)
+            acts[b, :, cols] = (
+                dot_nt(hidden[b, :, 0:half], down_v[0, cols, :])
+                + dot_nt(hidden[b, :, half : 2 * half], down_v[1, cols, :])
+            ).astype(jnp.bfloat16)
+            return carry
+
+        lax.fori_loop(0, width // tile, step, 0)
+
+    def d_copies(b):
+        return (
+            remote(part(b, dplane, lo), xd_in.at[b], d_send.at[0, b], d_recv.at[0, b], xp, tp),
+            remote(part(b, dplane, hi), yd_in.at[b], d_send.at[1, b], d_recv.at[1, b], yp, tp),
+        )
+
+    def g_copy(b, kind):
+        which, cols, box, to = (
+            (xplane, lo, xg_in, xp),
+            (xplane, hi, xg_in, xp),
+            (yplane, hi, yg_in, yp),
+            (yplane, lo, yg_in, yp),
+        )[kind]
+        return remote(
+            part(b, which, cols), box.at[b, :, cols], g_send.at[kind, b], g_recv.at[kind, b],
+            to, tp,
+        )
+
+    def first(b):
+        for copy in d_copies(b):
+            copy.start()
+        g_copy(b, 0).start()
+        g_copy(b, 2).start()
+
+    def add_into(ref, others):
+        total = ref[...].astype(jnp.float32)
+        for other in others:
+            total = total + other[...].astype(jnp.float32)
+        ref[...] = total.astype(jnp.bfloat16)
+
+    def combine(b):
+        x_copy, y_copy = d_copies(b)
+        x_copy.wait_recv()
+        add_into(part(b, yplane, lo), [xd_in.at[b]])
+        g_copy(b, 3).start()
+        y_copy.wait_recv()
+        add_into(part(b, xplane, hi), [yd_in.at[b]])
+        g_copy(b, 1).start()
+
+    every = pl.ds(0, width)
+
+    def z_copy(b, way):
+        box = (zb_in, za_in)[way]
+        return remote(
+            part(b, plane, every), box.at[b], z_send.at[way, b], z_recv.at[way, b],
+            fs + (4, -4)[way], tp,
+        )
+
+    def settle(b):
+        for kind in range(4):
+            g_copy(b, kind).wait_recv()
+        add_into(part(b, plane, every), [xg_in.at[b], yg_in.at[b]])
+        if b > 0:
+            pl.when(z == 0)(z_copy(b, 0).start)
+        if b < 3:
+            pl.when(z == 3)(z_copy(b, 1).start)
+
+    def relay(b):
+        if b > 0:
+            @pl.when(jnp.logical_and(z > 0, z < b))
+            def _():
+                z_copy(b, 0).wait_recv()
+                add_into(part(b, plane, every), [zb_in.at[b]])
+                z_copy(b, 0).start()
+
+        if b < 3:
+            @pl.when(jnp.logical_and(z < 3, z > b))
+            def _():
+                z_copy(b, 1).wait_recv()
+                add_into(part(b, plane, every), [za_in.at[b]])
+                z_copy(b, 1).start()
+
+    def finish(b):
+        @pl.when(z == b)
+        def _():
+            boxes = []
+            if b > 0:
+                z_copy(b, 0).wait_recv()
+                boxes.append(zb_in)
+            if b < 3:
+                z_copy(b, 1).wait_recv()
+                boxes.append(za_in)
+            for side in range(2):
+                cols = pl.ds(side * mid, mid)
+                total = acts[b, pl.ds(plane * share, share), cols].astype(jnp.float32)
+                for box in boxes:
+                    total = total + box[b, :, cols].astype(jnp.float32)
+                fin[side] = total.astype(jnp.bfloat16)
+
+    u0, u1, u2, u3 = UNITS
+    down_unit(u0)
+    first(u0)
+    chain.stage(4)
+    down_unit(u1)
+    first(u1)
+    combine(u0)
+    down_unit(u2)
+    first(u2)
+    combine(u1)
+    down_unit(u3)
+    first(u3)
+
+    chain.finish()
+    puts = [
+        pltpu.make_async_copy(
+            common.at[:, pl.ds(i * half, half)], ref, loc_sem.at[1 + i]
+        )
+        for i, ref in enumerate((common_gate, common_up, common_down))
+    ]
+    for copy in puts:
+        copy.start()
+
+    def shared_step(c, carry):
+        a = normed[...]
+        cols = pl.ds(pl.multiple_of(c * tile, tile), tile)
+        gate = jnp.dot(a, common[:, cols], preferred_element_type=jnp.float32)
+        up = jnp.dot(
+            a, common[:, pl.ds(pl.multiple_of(half + c * tile, tile), tile)],
+            preferred_element_type=jnp.float32,
+        )
+        shid[:, cols] = (jax.nn.silu(gate) * up).astype(jnp.bfloat16)
+        return carry
+
+    def shared_down_step(n, carry):
+        per = mid // tile
+        spart[n // per, :, pl.ds(pl.multiple_of((n % per) * tile, tile), tile)] = dot_nt(
+            shid[...],
+            common[pl.ds(pl.multiple_of(n * tile, tile), tile), 2 * half : 3 * half],
+        ).astype(jnp.bfloat16)
+        return carry
+
+    lax.fori_loop(0, per_half, shared_step, 0)
+    lax.fori_loop(0, width // tile, shared_down_step, 0)
+
+    settle(u0)
+    combine(u2)
+    settle(u1)
+    relay(u0)
+    s_copy = remote(
+        spart.at[1 - tp], spart_in, e_send.at[0], e_recv.at[0], fs, 1 - tp
+    )
+    s_copy.start()
+    combine(u3)
+    settle(u2)
+    relay(u1)
+    settle(u3)
+    relay(u2)
+    relay(u3)
+    for b in UNITS:
+        finish(b)
+    f_copy = remote(fin.at[1 - tp], fin_in, e_send.at[1], e_recv.at[1], fs, 1 - tp)
+    f_copy.start()
+    s_copy.wait()
+    near = pl.ds(pl.multiple_of(tp * share, share), share)
+    far = pl.ds(pl.multiple_of((1 - tp) * share, share), share)
+    f_copy.wait()
+    for where, value in ((near, fin[tp]), (far, fin_in[...])):
+        total = (
+            spart[tp, where, :].astype(jnp.float32)
+            + spart_in[where, :].astype(jnp.float32)
+            + value.astype(jnp.float32)
+        )
+        out_ref[where, :] = total.astype(jnp.bfloat16)
+
+    own_down.wait()
+
+    def wait_down(i, carry):
+        frm = ex.partner(i)
+        pltpu.make_async_copy(
+            ex.piece(down_v.at[0], frm), ex.piece(sample_down, frm), load_sem.at[0, frm]
+        ).wait()
+        return carry
+
+    lax.fori_loop(1, 16, wait_down, 0)
+    for copy in puts:
+        copy.wait()
+    chain.drain()
+    ex.drain()
+    for b in UNITS:
+        for copy in d_copies(b):
+            copy.wait_send()
+        for kind in range(4):
+            g_copy(b, kind).wait_send()
+        if b > 0:
+            pl.when(z < b)(z_copy(b, 0).wait_send)
+        if b < 3:
+            pl.when(z > b)(z_copy(b, 1).wait_send)
+
+
+HBM = pl.BlockSpec(memory_space=pl.ANY)
+VMEM = pl.BlockSpec(memory_space=pltpu.VMEM)
+DMA = pltpu.SemaphoreType.DMA
+
+
+def gather(tokens_share, dense, gain, raws):
+    experts, rows, half = raws[0].shape
+    share, width = tokens_share.shape
+    n = len(raws)
+    weight = jax.ShapeDtypeStruct((experts * rows, half), jnp.bfloat16)
+    return pl.pallas_call(
+        gather_kernel,
+        out_shape=[
+            jax.ShapeDtypeStruct((experts, share, width), jnp.bfloat16),
+            jax.ShapeDtypeStruct((experts, 1, share), jnp.float32),
+        ] + [weight] * (2 * n),
+        in_specs=[VMEM] * 3 + [HBM] * n,
+        out_specs=[HBM, VMEM] + [HBM] * (2 * n),
+        scratch_shapes=[
+            pltpu.VMEM((share, width), jnp.bfloat16),
+            pltpu.VMEM((n, experts, rows, half), jnp.float32),
+            pltpu.VMEM((n, experts, rows, half), jnp.bfloat16),
+            DMA((4, 4)), DMA((4,)), DMA((16,)), DMA((16,)), DMA((16,)),
+            DMA((n, 16)), DMA((n, 16)), DMA((n, 16)), DMA((n, 16)), DMA((n, 16)), DMA((4,)),
+        ],
+        compiler_params=pltpu.CompilerParams(
+            collective_id=1, has_side_effects=True, vmem_limit_bytes=32 << 20
+        ),
+        name="gather",
+    )(tokens_share, dense, gain, *raws)
+
+
+def mix(tokens, scale, gain, shared, gathered, weights, down):
+    experts, rows, half = down.shape
+    tok_rows, width = tokens.shape
+    share = tok_rows // 2
+    bf16 = jnp.bfloat16
+    weight = jax.ShapeDtypeStruct((experts * rows, half), bf16)
+    return pl.pallas_call(
+        mix_kernel,
+        out_shape=[jax.ShapeDtypeStruct((tok_rows, width // 2), bf16)] + [weight] * 4,
+        in_specs=[VMEM] * 6 + [HBM] * 6,
+        out_specs=[VMEM] + [HBM] * 4,
+        scratch_shapes=[
+            pltpu.VMEM((4, 4 * share, width), bf16),
+            pltpu.VMEM((2, 2, width, half), bf16),
+            pltpu.VMEM((2, width, half), bf16),
+            pltpu.VMEM((1, experts, rows, half), jnp.float32),
+            pltpu.VMEM((1, experts, rows, half), bf16),
+            pltpu.VMEM((4, 4 * share, 2 * half), bf16),
+            pltpu.VMEM((width, 3 * half), bf16),
+            pltpu.VMEM((tok_rows, width), bf16),
+            pltpu.VMEM((tok_rows, half), bf16),
+            pltpu.VMEM((2, tok_rows, width // 2), bf16),
+            pltpu.VMEM((tok_rows, width // 2), bf16),
+            pltpu.VMEM((2, share, width // 2), bf16),
+            pltpu.VMEM((share, width // 2), bf16),
+            pltpu.VMEM((4, share, width // 2), bf16),
+            pltpu.VMEM((4, share, width // 2), bf16),
+            pltpu.VMEM((4, share, width), bf16),
+            pltpu.VMEM((4, share, width), bf16),
+            pltpu.VMEM((4, share, width), bf16),
+            pltpu.VMEM((4, share, width), bf16),
+            DMA((4, 4)), DMA((4,)), DMA((16,)),
+            DMA((1, 16)), DMA((1, 16)), DMA((1, 16)), DMA((1, 16)), DMA((1, 16)),
+            DMA((2, 4)), DMA((2, 4)), DMA((4, 4)), DMA((4, 4)), DMA((2, 4)), DMA((2, 4)),
+            DMA((2,)), DMA((2,)), DMA((8,)),
+        ],
+        compiler_params=pltpu.CompilerParams(
+            collective_id=2, has_side_effects=True, vmem_limit_bytes=67043328
+        ),
+        name="mix",
+    )(tokens, scale, gain, *shared, gathered, *weights, down)
 
 
 def ring_of(fs_count):
@@ -28,7 +662,7 @@
     return jnp.concatenate([blocks[i : i + 1] for i in order], axis=0)
 
 
-def body(
+def general_body(
     tokens,
     routes,
     route_weights,
@@ -137,8 +771,38 @@
     layer_output = (routed.astype(jnp.float32) + shared_sum).astype(jnp.bfloat16)
     return (layer_output, sample_gate, sample_up, sample_down, common_gate, common_up, common_down)
 
+def block_body(
+    tokens, routes, route_weights, norm_gain,
+    expert_gate, expert_up, expert_down,
+    shared_gate, shared_up, shared_down,
+):
+    tp_index = lax.axis_index("tp")
+    tok_rows, width = tokens.shape
+    experts = expert_gate.shape[0]
+    share = tok_rows // 2
+    own_routes = lax.dynamic_slice_in_dim(routes, tp_index * share, share, 0)
+    own_weights = lax.dynamic_slice_in_dim(route_weights, tp_index * share, share, 0)
+    own_tokens = lax.dynamic_slice_in_dim(tokens, tp_index * share, share, 0)
+    member = own_routes[None, :, :] == jnp.arange(experts, dtype=jnp.int32)[:, None, None]
+    dense = jnp.sum(jnp.where(member, own_weights[None, :, :], 0.0), axis=2)
+    gain = norm_gain[:, None]
+    gathered, scale, gate_own, up_own, gate_other, up_other = gather(
+        own_tokens, dense[:, None, :], gain, (expert_gate, expert_up)
+    )
+    layer_output, sample_down, common_gate, common_up, common_down = mix(
+        tokens, scale.reshape(experts * share, 1), gain,
+        (shared_gate, shared_up, shared_down), gathered.reshape(experts * share, width),
+        (gate_own, up_own, gate_other, up_other), expert_down,
+    )
+    return (
+        layer_output, gate_own[None], up_own[None], sample_down[None],
+        common_gate, common_up, common_down,
+    )
+
 
 def solution(mesh):
+    fits = mesh.shape["fs"] == 16 and mesh.shape["tp"] == 2
+    body = block_body if fits else general_body
     return jax.shard_map(
         body,
         mesh=mesh,

time: 482 us -> 378 us (0.78)
  Pallas kernels: 0 us -> 347 us
  waiting for transfers between devices: 209 us -> 0 us
  blocking collectives: 124 us -> 0 us
  matrix products: 57.7 us -> 0 us
  starting transfers between devices: 19.7 us -> 0 us
  other arithmetic: 17.1 us -> 0.01 us
  between operations: 14.1 us -> 0.71 us
  local copies, waits for them, and re-layouts: 37.6 us -> 30 us
    pallas_call x0 -> x2, Pallas kernels: none -> 347 us  [the longest x1 214 us: mix(): pl.pallas_call(mix_kernel, out_shape=[jax.ShapeDtypeStruct((tok_rows, wid...]
    all_to_all x2 -> x0, waiting for transfers between devices: 143 us -> none  [the longest x1 84.8 us: body(): lax.all_to_all(rounded[1], 'fs', split_axis=0, concat_axis=1, tiled=True)]
    all_to_all x3 -> x0, blocking collectives: 96.5 us -> none  [the longest x1 87.8 us: body(): lax.all_to_all(rounded[0], 'fs', split_axis=0, concat_axis=1, tiled=True)]
    reduce_scatter x1 -> x0, waiting for transfers between devices: 66 us -> none  [body(): lax.psum_scatter(total.astype(jnp.bfloat16), 'fs', scatter_dimension=0, t...]
    dot_general x7 -> x0, matrix products: 57.7 us -> none  [the longest x2 30.2 us: body(): jnp.einsum('rf,df->rd', hidden, down_w, preferred_element_type=jnp.float32)]
    all_gather x1 -> x0, blocking collectives: 28 us -> none  [body(): dense_all = lax.all_gather(dense, 'fs', axis=0, tiled=False)]
    convert_element_type x6 -> x0, other arithmetic: 14.6 us -> none  [the longest x1 6.12 us: body(): (expert_up * gain_rows).astype(jnp.bfloat16)]
    all_to_all x2 -> x0, starting transfers between devices: 13.1 us -> none  [the longest x1 7.48 us: body(): lax.all_to_all(rounded[2], 'fs', split_axis=0, concat_axis=1, tiled=True)]
  transfers between devices with their start and end apart: 8 -> 0, of which waited for: 3 -> 0; matrix products, arithmetic and copies ran while one was open for 20% -> 0% of each run, Pallas kernels for 0% -> 0%
where the time goes in v2:
time: 378 us
  Pallas kernels  347 us (92%)
  local copies, waits for them, and re-layouts  30 us (8%)
    pallas_call x1, Pallas kernels, mix(): pl.pallas_call(mix_kernel, out_shape=[jax.ShapeDtypeStruct((tok_rows, wid...  214 us
    pallas_call x1, Pallas kernels, gather(): pl.pallas_call(gather_kernel, out_shape=[jax.ShapeDtypeStruct((experts, s...  133 us
    unnamed x31, local copies, waits for them, and re-layouts  25.4 us

profile of v2, /device:TPU:9, one launch (start us, length us, event | category | flops | bytes accessed | tf_op | source)
XLA Modules:
  0.0 377.9 jit_solution(3136968500989257611)
XLA Ops:
  0.6 0.7 constant_dynamic-slice_fusion.1
  1.3 0.7 constant_dynamic-slice_fusion
  2.0 0.8 copy.26.gain_ref
  2.8 1.1 constant_dynamic-slice_fusion.2.tok_ref
  3.9 2.2 copy-done.3
  6.1 2.2 copy-done.4
  8.3 133.1 %gather.1 = (bf16[16,128,2048]{2,1,0:T(8,128)(2,1)}, f32[16,1,128]{2,1,0:T(1,128)S(1)}, bf16[2048,512]{1,0:T(8,128)(2,1)S(1)}, bf16[2048,512]{1,0:T(8,128)(2,1)S...) custom-call(bf16[128,2048]{1,0:T(8,128)(2,1)S(1)} %constant_dynamic-slice_fusion.2.tok_ref, ...), custom_call_target="tpu_custom_call" | custom-call | tf_op jit(solution)/shard_map/gather/pallas_call | solution.py:584
  141.5 1.3 copy-done
  142.8 1.3 copy-done.2
  144.1 1.3 copy-done.5
  145.4 1.3 copy-done.6
  146.7 1.3 copy.27.scale_ref
  148.1 214.1 %mix.1 = (bf16[256,1024]{1,0:T(8,128)(2,1)}, bf16[2048,512]{1,0:T(8,128)(2,1)}, bf16[2048,512]{1,0:T(8,128)(2,1)}, bf16[2048,512]{1,0:T(8,128)(2,1)}, bf16[2048,512]{1,0:T(8,128)(2,1)}) custom-call(bf16[256,2048]{1,0:T(8,128)(2,1)} %tok_ref.1, f32[2048,1]{1,0:T(8,128)} %copy.27.scale_ref, f32[128,1]{1,0:T(8,128)} %copy-done.7, f32[128,512]{1,0:T(8,128)} %sgate_ref.1, ...), custom_call_target="tpu_custom_call" | custom-call | tf_op jit(solution)/shard_map/mix/pallas_call | solution.py:612
  362.1 1.9 copy.36
  364.0 3.2 copy.37
  367.2 1.3 copy.38
  368.5 1.0 copy-done.11
  369.6 1.3 copy.39
  370.9 1.0 copy-done.10
  371.9 1.3 copy.40
  373.2 1.0 copy-done.9
  374.3 1.3 copy.41
  375.6 1.0 copy-done.8
  376.6 1.3 copy.42
  (15 shorter events, 0.0 us)
Async XLA Ops:
  2.8 138.6 %copy-start.7 = (f32[128,1]{1,0:T(8,128)}, f32[128,1]{1,0:T(8,128)S(1)}, u32[]{:S(2)}) copy-start(f32[128,1]{1,0:T(8,128)S(1)} %copy.26.gain_ref) | copy-start | bytes 1540
  3.9 2.2 copy-start.3
  6.1 2.2 copy-start.4
  141.5 1.3 copy-start
  142.8 1.3 copy-start.2
  144.1 1.3 copy-start.5
  145.4 1.3 copy-start.6
  364.0 3.2 copy-start.1
  367.2 2.3 copy-start.11
  369.6 2.3 copy-start.10
  371.9 2.3 copy-start.9
  374.3 2.3 copy-start.8

commit v3 on v0

--- a/solution.py
+++ b/solution.py
@@ -1,15 +1,643 @@
+import functools
+
 import jax
 import jax.numpy as jnp
 from jax import lax
+from jax.experimental import pallas as pl
+from jax.experimental.pallas import tpu as pltpu
 from jax.sharding import PartitionSpec as P
 
+MESH = pl.DeviceIdType.MESH
 EPSILON = 1e-06
+UNITS = (0, 3, 1, 2)
 
 
 def normalize(tokens):
     values = tokens.astype(jnp.float32)
     scale = lax.rsqrt(jnp.mean(values * values, axis=-1, keepdims=True) + EPSILON)
     return (values * scale).astype(jnp.bfloat16)
+
+
+def place():
+    fs = lax.axis_index("fs")
+    return fs, lax.axis_index("tp"), fs % 2, (fs // 2) % 2, fs // 4
+
+
+def barrier_all(fs, tp):
+    count = lax.axis_size("fs")
+    sem = pltpu.get_barrier_semaphore()
+    for step in range(1, count):
+        pl.semaphore_signal(
+            sem, inc=1, device_id=((fs + step) % count, tp), device_id_type=MESH
+        )
+    pl.semaphore_signal(sem, inc=1, device_id=(fs, 1 - tp), device_id_type=MESH)
+    pl.semaphore_wait(sem, count)
+
+
+def column(row):
+    return jnp.transpose(jnp.broadcast_to(row, (row.shape[1], row.shape[1])))[:, 0:1]
+
+
+def remote(src, dst, ssem, rsem, to, core):
+    return pltpu.make_async_remote_copy(
+        src_ref=src, dst_ref=dst, send_sem=ssem, recv_sem=rsem,
+        device_id=(to, core), device_id_type=MESH,
+    )
+
+
+class Chain:
+    def __init__(self, at, send_sem, fwd_sem, recv_sem):
+        self.fs, self.tp, self.x, self.y, self.z = place()
+        self.at, self.send_sem, self.fwd_sem, self.recv_sem = at, send_sem, fwd_sem, recv_sem
+        self.plane = self.fs % 4
+        self.xp, self.yp = self.fs + 1 - 2 * self.x, self.fs + 2 - 4 * self.y
+        self.xplane, self.yplane = self.plane + 1 - 2 * self.x, self.plane + 2 - 4 * self.y
+
+    def copy(self, slot, sem, to):
+        here = self.at(slot)
+        return remote(here, here, sem, self.recv_sem.at[slot], to, self.tp)
+
+    def line(self, block, kind):
+        z = self.z
+        cond = (
+            jnp.logical_and(z < 3, block <= z), jnp.logical_and(z > 0, block >= z), None, None
+        )[kind]
+        to = (self.fs + 4, self.fs - 4, self.xp, self.yp)[kind]
+        return cond, self.copy(block * 4 + self.plane, self.send_sem.at[kind, block], to)
+
+    def spread(self, block, kinds=(0, 1, 2, 3)):
+        for kind in kinds:
+            cond, copy = self.line(block, kind)
+            if cond is None:
+                copy.start()
+            else:
+                pl.when(cond)(copy.start)
+
+    def landed(self, slot):
+        self.copy(slot, self.send_sem.at[0, 0], self.xp).wait_recv()
+
+    def arrive(self, block, kinds):
+        self.landed(block * 4 + self.plane)
+        self.spread(block, kinds)
+
+    def forward_copy(self, block, low):
+        slot = block * 4 + (self.xplane if low else self.yplane)
+        return self.copy(slot, self.fwd_sem.at[block], self.yp if low else self.xp)
+
+    def plane_forward(self, block):
+        def forward(low):
+            copy = self.forward_copy(block, low)
+            copy.wait_recv()
+            copy.start()
+
+        if isinstance(block, int):
+            forward(block < 2)
+            return
+        pl.when(jnp.logical_and(block >= 0, block < 2))(lambda: forward(True))
+        pl.when(jnp.logical_and(block >= 2, block < 4))(lambda: forward(False))
+
+    def hop(self, step, kinds=(0, 1, 2, 3)):
+        z = self.z
+        pl.when(z - step - 1 >= 0)(lambda: self.arrive(z - step - 1, kinds))
+        pl.when(z + step + 1 < 4)(lambda: self.arrive(z + step + 1, kinds))
+
+    def turn(self, step):
+        self.plane_forward(self.z - step)
+        if step > 0:
+            self.plane_forward(self.z + step)
+
+    def finish(self):
+        for block in range(4):
+            self.landed(block * 4 + (self.yplane if block < 2 else self.xplane))
+            self.landed(block * 4 + 3 - self.plane)
+
+    def drain(self):
+        for block in range(4):
+            for kind in range(4):
+                cond, copy = self.line(block, kind)
+                if cond is None:
+                    copy.wait_send()
+                else:
+                    pl.when(cond)(copy.wait_send)
+            self.forward_copy(block, block < 2).wait_send()
+
+
+class Exchange:
+    def __init__(self, raw, wide, narrow, own, other, sems):
+        self.raw, self.wide, self.narrow, self.own, self.other = raw, wide, narrow, own, other
+        self.load_sem, self.send_sem, self.recv_sem, self.psend, self.precv = sems
+        self.fs, self.tp, self.x, self.y, self.z = place()
+        self.rows = raw[0].shape[1]
+
+    def partner(self, dz, turn, sign=1):
+        return (
+            ((self.z + 4 + sign * dz) % 4) * 4
+            + ((self.y + turn // 2) % 2) * 2
+            + (self.x + turn % 2) % 2
+        )
+
+    def load(self, t, to):
+        return pltpu.make_async_copy(
+            self.raw[t].at[to], self.wide.at[to], self.load_sem.at[t, to]
+        )
+
+    def each(self, lower, upper, body, sign=1):
+        def near(i, carry):
+            body(self.partner(0, i, sign))
+            return carry
+
+        def far(i, carry):
+            k = i - 4
+            body(self.partner(1 + (k + 1) % 3, k // 3, sign))
+            return carry
+
+        if lower < 4:
+            lax.fori_loop(lower, min(upper, 4), near, 0)
+        if upper > 4:
+            lax.fori_loop(max(lower, 4), min(upper, 16), far, 0)
+        if upper > 16:
+            body(self.fs)
+
+    def convert(self, t, gain):
+        def one(to):
+            self.load(t, to).wait()
+            block = self.wide[to]
+            if gain is not None:
+                block = block * gain
+            self.narrow[t, to] = block.astype(jnp.bfloat16)
+            if t + 1 < len(self.raw):
+                self.load(t + 1, to).start()
+
+        self.each(1, 17, one)
+
+    def piece(self, ref, frm):
+        return ref.at[pl.ds(frm * self.rows, self.rows)]
+
+    def copy(self, t, to):
+        return remote(
+            self.narrow.at[t, to], self.piece(self.own[t], self.fs),
+            self.send_sem.at[t, to], self.recv_sem.at[t, self.fs], to, self.tp,
+        )
+
+    def send(self, lower, upper, tensors):
+        def one(to):
+            for t in tensors:
+                self.copy(t, to).start()
+
+        self.each(lower, upper, one)
+
+    def across(self, t, frm, src):
+        return remote(
+            src, self.piece(self.other[t], frm), self.psend.at[t, frm], self.precv.at[t, frm],
+            self.fs, 1 - self.tp,
+        )
+
+    def keep(self, tensors):
+        for t in tensors:
+            self.own[t][pl.ds(self.fs * self.rows, self.rows), :] = self.narrow[t, self.fs]
+            self.across(t, self.fs, self.narrow.at[t, self.fs]).start()
+
+    def pass_on(self, tensors, lower=1, upper=16):
+        def one(frm):
+            for t in tensors:
+                piece = self.piece(self.own[t], frm)
+                remote(
+                    piece, piece, self.send_sem.at[t, frm], self.recv_sem.at[t, frm], frm, self.tp
+                ).wait_recv()
+                self.across(t, frm, piece).start()
+
+        self.each(lower, upper, one, -1)
+
+    def finish(self, tensors):
+        def one(frm):
+            for t in tensors:
+                self.across(t, frm, self.piece(self.own[t], frm)).wait()
+
+        self.each(1, 17, one, -1)
+
+    def drain(self):
+        def one(to):
+            for t in range(len(self.raw)):
+                self.copy(t, to).wait_send()
+
+        self.each(1, 16, one)
+
+
+def dot_nt(a, b):
+    return lax.dot_general(a, b, (((1,), (1,)), ((), ())), preferred_element_type=jnp.float32)
+
+
+def whole_kernel(
+    tok_ref, scale_ref, gain_ref, sgate_ref, sup_ref, sdown_ref, gate_ref, up_ref, down_ref,
+    out_ref, sample_gate, sample_up, sample_down, common_gate, common_up, common_down,
+    acts, gate_up, down_v, wide, narrow, hidden, common, normed, scales, scol,
+    shid, spart, spart_in, fin, fin_in, xd_in, yd_in, xg_in, yg_in, zb_in, za_in,
+    t_send, t_fwd, t_recv, c_send, c_fwd, c_recv, sc_send, sc_recv,
+    load_sem, w_send, w_recv, p_send, p_recv,
+    d_send, d_recv, g_send, g_recv, z_send, z_recv, e_send, e_recv, loc_sem,
+):
+    fs, tp, x, y, z = place()
+    rows, half = sgate_ref.shape
+    width = tok_ref.shape[1]
+    share = acts.shape[1] // 4
+    ex = Exchange(
+        (gate_ref, up_ref, down_ref), wide, narrow,
+        (gate_up.at[0, 0], gate_up.at[1, 0], down_v.at[0]),
+        (gate_up.at[0, 1], gate_up.at[1, 1], down_v.at[1]),
+        (load_sem, w_send, w_recv, p_send, p_recv),
+    )
+    tokens = Chain(
+        lambda slot: acts.at[slot // 4, pl.ds((slot % 4) * share, share)], t_send, t_fwd, t_recv
+    )
+    chain = Chain(lambda slot: common.at[pl.ds(slot * rows, rows)], c_send, c_fwd, c_recv)
+
+    ex.each(1, 17, lambda to: ex.load(0, to).start())
+    gain = column(gain_ref[...])
+    mine = pl.ds(fs * rows, rows)
+    common[mine, 0:half] = (sgate_ref[...] * gain).astype(jnp.bfloat16)
+    common[mine, half : 2 * half] = (sup_ref[...] * gain).astype(jnp.bfloat16)
+    common[mine, 2 * half : 3 * half] = sdown_ref[...].astype(jnp.bfloat16)
+    normed[...] = normalize(tok_ref[...])
+    acts[z, pl.ds((fs % 4) * share, share), :] = normed[
+        pl.ds(pl.multiple_of(tp * share, share), share), :
+    ]
+    ex.convert(0, gain)
+    ex.convert(1, gain)
+    ex.convert(2, None)
+    barrier_all(fs, tp)
+
+    tokens.spread(z)
+
+    def scale_copy(to):
+        return remote(
+            scale_ref.at[to, tp], scales.at[fs], sc_send.at[to], sc_recv.at[fs], to, tp
+        )
+
+    own_scale = pltpu.make_async_copy(scale_ref.at[fs, tp], scales.at[fs], loc_sem.at[0])
+    own_scale.start()
+    ex.each(1, 16, lambda to: scale_copy(to).start())
+    ex.send(1, 5, (0, 1))
+    tokens.hop(0)
+    tokens.turn(0)
+    ex.send(5, 6, (0, 1))
+    tokens.hop(1)
+    tokens.turn(1)
+    tokens.hop(2)
+    along = (0, 1)
+    chain.spread(z, along)
+    ex.send(6, 9, (0, 1))
+    tokens.turn(2)
+    chain.hop(0, along)
+    ex.send(9, 12, (0, 1))
+    chain.hop(1, along)
+    ex.send(12, 16, (0, 1))
+    ex.send(4, 16, (2,))
+    tokens.turn(3)
+    chain.hop(2, along)
+    ex.send(1, 4, (2,))
+    for block in range(4):
+        chain.spread(block, (2, 3))
+    ex.keep((0, 1, 2))
+    own_scale.wait()
+
+    def take_scale(frm):
+        here = scales.at[frm]
+        remote(here, here, sc_send.at[frm], sc_recv.at[frm], frm, tp).wait_recv()
+        scale_copy(frm).wait_send()
+
+    ex.each(1, 16, take_scale)
+    for slot in range(16):
+        scol[pl.ds(slot * share, share), :] = column(scales[slot])
+    ex.pass_on((0, 1))
+    ex.finish((0, 1))
+    samples = [
+        pltpu.make_async_copy(gate_up.at[t, 0], ref, loc_sem.at[1 + t])
+        for t, ref in enumerate((sample_gate, sample_up))
+    ]
+    for copy in samples:
+        copy.start()
+    tokens.finish()
+
+    tile = 256
+    per_half = half // tile
+
+    def gate_up_unit(b):
+        def step(j, carry):
+            h, c = j // per_half, j % per_half
+            cols = pl.ds(pl.multiple_of(c * tile, tile), tile)
+            a = acts[b]
+            gate = jnp.dot(a, gate_up[0, h, :, cols], preferred_element_type=jnp.float32)
+            up = jnp.dot(a, gate_up[1, h, :, cols], preferred_element_type=jnp.float32)
+            scale = scol[pl.ds(b * 4 * share, 4 * share), :]
+            hidden[b, :, pl.ds(pl.multiple_of(j * tile, tile), tile)] = (
+                jax.nn.silu(gate) * up * scale
+            ).astype(jnp.bfloat16)
+            return carry
+
+        lax.fori_loop(0, 2 * per_half, step, 0)
+
+    for b in UNITS:
+        gate_up_unit(b)
+    tokens.drain()
+    chain.plane_forward(0)
+    chain.plane_forward(1)
+
+    ex.pass_on((2,))
+    ex.finish((2,))
+    samples.append(pltpu.make_async_copy(down_v.at[0], sample_down, loc_sem.at[3]))
+    samples[-1].start()
+
+    plane = fs % 4
+    xp, yp = chain.xp, chain.yp
+    xplane, yplane, dplane = chain.xplane, chain.yplane, 3 - plane
+    mid, quarter = width // 2, width // 4
+
+    def columns(side):
+        return pl.ds(side * mid, quarter), pl.ds(side * mid + quarter, quarter)
+
+    def part(b, which, cols):
+        return acts.at[b, pl.ds(which * share, share), cols]
+
+    def down_unit(b, side):
+        def step(n, carry):
+            cols = pl.ds(pl.multiple_of(side * mid + n * tile, tile), tile)
+            acts[b, :, cols] = (
+                dot_nt(hidden[b, :, 0:half], down_v[0, cols, :])
+                + dot_nt(hidden[b, :, half : 2 * half], down_v[1, cols, :])
+            ).astype(jnp.bfloat16)
+            return carry
+
+        lax.fori_loop(0, mid // tile, step, 0)
+
+    def d_copies(b, side):
+        lo, hi = columns(side)
+        box = pl.ds(side * quarter, quarter)
+        n = 2 * b + side
+        return (
+            remote(
+                part(b, dplane, lo), xd_in.at[b, :, box], d_send.at[0, n], d_recv.at[0, n], xp, tp
+            ),
+            remote(
+                part(b, dplane, hi), yd_in.at[b, :, box], d_send.at[1, n], d_recv.at[1, n], yp, tp
+            ),
+        )
+
+    def g_copy(b, side, kind):
+        lo, hi = columns(side)
+        which, cols, box, to = (
+            (xplane, lo, xg_in, xp),
+            (xplane, hi, xg_in, xp),
+            (yplane, hi, yg_in, yp),
+            (yplane, lo, yg_in, yp),
+        )[kind]
+        n = 2 * b + side
+        return remote(
+            part(b, which, cols), box.at[b, :, cols], g_send.at[kind, n], g_recv.at[kind, n],
+            to, tp,
+        )
+
+    def first(b, side):
+        for copy in d_copies(b, side):
+            copy.start()
+        g_copy(b, side, 0).start()
+        g_copy(b, side, 2).start()
+
+    def add_into(ref, others):
+        total = ref[...].astype(jnp.float32)
+        for other in others:
+            total = total + other[...].astype(jnp.float32)
+        ref[...] = total.astype(jnp.bfloat16)
+
+    def combine(b, side):
+        lo, hi = columns(side)
+        box = pl.ds(side * quarter, quarter)
+        x_copy, y_copy = d_copies(b, side)
+        x_copy.wait_recv()
+        add_into(part(b, yplane, lo), [xd_in.at[b, :, box]])
+        g_copy(b, side, 3).start()
+        y_copy.wait_recv()
+        add_into(part(b, xplane, hi), [yd_in.at[b, :, box]])
+        g_copy(b, side, 1).start()
+
+    def z_copy(b, side, way):
+        box = (zb_in, za_in)[way]
+        cols = pl.ds(side * mid, mid)
+        n = 2 * b + side
+        return remote(
+            part(b, plane, cols), box.at[b, :, cols], z_send.at[way, n], z_recv.at[way, n],
+            fs + (4, -4)[way], tp,
+        )
+
+    def settle(b, side):
+        cols = pl.ds(side * mid, mid)
+        for kind in range(4):
+            g_copy(b, side, kind).wait_recv()
+        add_into(part(b, plane, cols), [xg_in.at[b, :, cols], yg_in.at[b, :, cols]])
+        if b > 0:
+            pl.when(z == 0)(z_copy(b, side, 0).start)
+        if b < 3:
+            pl.when(z == 3)(z_copy(b, side, 1).start)
+
+    def relay(b, side):
+        cols = pl.ds(side * mid, mid)
+        if b > 0:
+            @pl.when(jnp.logical_and(z > 0, z < b))
+            def _():
+                z_copy(b, side, 0).wait_recv()
+                add_into(part(b, plane, cols), [zb_in.at[b, :, cols]])
+                z_copy(b, side, 0).start()
+
+        if b < 3:
+            @pl.when(jnp.logical_and(z < 3, z > b))
+            def _():
+                z_copy(b, side, 1).wait_recv()
+                add_into(part(b, plane, cols), [za_in.at[b, :, cols]])
+                z_copy(b, side, 1).start()
+
+    def finish(b):
+        @pl.when(z == b)
+        def _():
+            for side in range(2):
+                cols = pl.ds(side * mid, mid)
+                total = acts[b, pl.ds(plane * share, share), cols].astype(jnp.float32)
+                if b > 0:
+                    z_copy(b, side, 0).wait_recv()
+                    total = total + zb_in[b, :, cols].astype(jnp.float32)
+                if b < 3:
+                    z_copy(b, side, 1).wait_recv()
+                    total = total + za_in[b, :, cols].astype(jnp.float32)
+                fin[side] = total.astype(jnp.bfloat16)
+
+    puts = [
+        pltpu.make_async_copy(common.at[:, pl.ds(i * half, half)], ref, loc_sem.at[4 + i])
+        for i, ref in enumerate((common_gate, common_up, common_down))
+    ]
+
+    def shared_step(c, carry):
+        a = normed[...]
+        cols = pl.ds(pl.multiple_of(c * tile, tile), tile)
+        gate = jnp.dot(a, common[:, cols], preferred_element_type=jnp.float32)
+        up = jnp.dot(
+            a, common[:, pl.ds(pl.multiple_of(half + c * tile, tile), tile)],
+            preferred_element_type=jnp.float32,
+        )
+        shid[:, cols] = (jax.nn.silu(gate) * up).astype(jnp.bfloat16)
+        return carry
+
+    def shared_down_step(n, carry):
+        per = mid // tile
+        spart[n // per, :, pl.ds(pl.multiple_of((n % per) * tile, tile), tile)] = dot_nt(
+            shid[...],
+            common[pl.ds(pl.multiple_of(n * tile, tile), tile), 2 * half : 3 * half],
+        ).astype(jnp.bfloat16)
+        return carry
+
+    s_copy = remote(spart.at[1 - tp], spart_in, e_send.at[0], e_recv.at[0], fs, 1 - tp)
+
+    def shared_expert():
+        chain.finish()
+        for copy in puts:
+            copy.start()
+        lax.fori_loop(0, per_half, shared_step, 0)
+        lax.fori_loop(0, width // tile, shared_down_step, 0)
+        s_copy.start()
+
+    pieces = [(b, side) for b in UNITS for side in range(2)]
+    count = len(pieces)
+    for i in range(count + 4):
+        if i < count:
+            down_unit(*pieces[i])
+            first(*pieces[i])
+        if i == 1:
+            chain.plane_forward(2)
+        if i == 2:
+            chain.plane_forward(3)
+        if i == count + 1:
+            shared_expert()
+        if 1 <= i <= count:
+            combine(*pieces[i - 1])
+        if 2 <= i <= count + 1:
+            settle(*pieces[i - 2])
+        if i >= 4:
+            relay(*pieces[i - 4])
+    for b in UNITS:
+        finish(b)
+    f_copy = remote(fin.at[1 - tp], fin_in, e_send.at[1], e_recv.at[1], fs, 1 - tp)
+    f_copy.start()
+    s_copy.wait()
+    near = pl.ds(pl.multiple_of(tp * share, share), share)
+    far = pl.ds(pl.multiple_of((1 - tp) * share, share), share)
+    f_copy.wait()
+    for where, value in ((near, fin[tp]), (far, fin_in[...])):
+        total = (
+            spart[tp, where, :].astype(jnp.float32)
+            + spart_in[where, :].astype(jnp.float32)
+            + value.astype(jnp.float32)
+        )
+        out_ref[where, :] = total.astype(jnp.bfloat16)
+
+    for copy in samples:
+        copy.wait()
+    for copy in puts:
+        copy.wait()
+    chain.drain()
+    ex.drain()
+    for b, side in pieces:
+        for copy in d_copies(b, side):
+            copy.wait_send()
+        for kind in range(4):
+            g_copy(b, side, kind).wait_send()
+        if b > 0:
+            pl.when(z < b)(z_copy(b, side, 0).wait_send)
+        if b < 3:
+            pl.when(z > b)(z_copy(b, side, 1).wait_send)
+
+
+HBM = pl.BlockSpec(memory_space=pl.ANY)
+VMEM = pl.BlockSpec(memory_space=pltpu.VMEM)
+DMA = pltpu.SemaphoreType.DMA
+
+
+def whole(tokens, scale, gain, shared, raw):
+    experts, rows, half = raw[0].shape
+    tok_rows, width = tokens.shape
+    share = tok_rows // 2
+    bf16, f32 = jnp.bfloat16, jnp.float32
+    weight = jax.ShapeDtypeStruct((experts * rows, half), bf16)
+    return pl.pallas_call(
+        whole_kernel,
+        out_shape=[jax.ShapeDtypeStruct((tok_rows, width // 2), bf16)] + [weight] * 6,
+        in_specs=[VMEM] * 6 + [HBM] * 3,
+        out_specs=[VMEM] + [HBM] * 6,
+        scratch_shapes=[
+            pltpu.VMEM((4, 4 * share, width), bf16),
+            pltpu.VMEM((2, 2, width, half), bf16),
+            pltpu.VMEM((2, width, half), bf16),
+            pltpu.VMEM((experts, rows, half), f32),
+            pltpu.VMEM((3, experts, rows, half), bf16),
+            pltpu.VMEM((4, 4 * share, 2 * half), bf16),
+            pltpu.VMEM((width, 3 * half), bf16),
+            pltpu.VMEM((tok_rows, width), bf16),
+            pltpu.VMEM((experts, 1, share), f32),
+            pltpu.VMEM((experts * share, 1), f32),
+            pltpu.VMEM((tok_rows, half), bf16),
+            pltpu.VMEM((2, tok_rows, width // 2), bf16),
+            pltpu.VMEM((tok_rows, width // 2), bf16),
+            pltpu.VMEM((2, share, width // 2), bf16),
+            pltpu.VMEM((share, width // 2), bf16),
+            pltpu.VMEM((4, share, width // 2), bf16),
+            pltpu.VMEM((4, share, width // 2), bf16),
+            pltpu.VMEM((4, share, width), bf16),
+            pltpu.VMEM((4, share, width), bf16),
+            pltpu.VMEM((4, share, width), bf16),
+            pltpu.VMEM((4, share, width), bf16),
+            DMA((4, 4)), DMA((4,)), DMA((16,)), DMA((4, 4)), DMA((4,)), DMA((16,)),
+            DMA((16,)), DMA((16,)),
+            DMA((3, 16)), DMA((3, 16)), DMA((3, 16)), DMA((3, 16)), DMA((3, 16)),
+            DMA((2, 8)), DMA((2, 8)), DMA((4, 8)), DMA((4, 8)), DMA((2, 8)), DMA((2, 8)),
+            DMA((2,)), DMA((2,)), DMA((8,)),
+        ],
+        compiler_params=pltpu.CompilerParams(
+            collective_id=1, has_side_effects=True, vmem_limit_bytes=67043328
+        ),
+        name="whole",
+    )(tokens, scale, gain, *shared, *raw)
+
+
+def emit_kernel(count, *refs):
+    source, target, boxes = refs[:count], refs[count : 2 * count], refs[2 * count : -2]
+    in_sem, out_sem = refs[-2:]
+    parts = []
+    for i in range(count):
+        length = source[i].shape[0] // 4
+        for c in range(4):
+            at = pl.ds(c * length, length)
+            parts.append((
+                pltpu.make_async_copy(source[i].at[at], boxes[i].at[at], in_sem.at[i, c]),
+                pltpu.make_async_copy(boxes[i].at[at], target[i].at[at], out_sem.at[i, c]),
+            ))
+    for load, _ in parts:
+        load.start()
+    for load, store in parts:
+        load.wait()
+        store.start()
+    for _, store in parts:
+        store.wait()
+
+
+def emit(*arrays):
+    n = len(arrays)
+    shapes = [jax.ShapeDtypeStruct(a.shape, a.dtype) for a in arrays]
+    return pl.pallas_call(
+        functools.partial(emit_kernel, n),
+        out_shape=shapes,
+        in_specs=[HBM] * n,
+        out_specs=[HBM] * n,
+        scratch_shapes=[pltpu.VMEM(a.shape, a.dtype) for a in arrays]
+        + [DMA((n, 4)), DMA((n, 4))],
+        compiler_params=pltpu.CompilerParams(vmem_limit_bytes=67043328),
+        name="emit",
+    )(*arrays)
 
 
 def ring_of(fs_count):
@@ -28,7 +656,7 @@
     return jnp.concatenate([blocks[i : i + 1] for i in order], axis=0)
 
 
-def body(
+def general_body(
     tokens,
     routes,
     route_weights,
@@ -137,8 +765,33 @@
     layer_output = (routed.astype(jnp.float32) + shared_sum).astype(jnp.bfloat16)
     return (layer_output, sample_gate, sample_up, sample_down, common_gate, common_up, common_down)
 
+def block_body(
+    tokens, routes, route_weights, norm_gain,
+    expert_gate, expert_up, expert_down,
+    shared_gate, shared_up, shared_down,
+):
+    tok_rows = tokens.shape[0]
+    experts = expert_gate.shape[0]
+    share = tok_rows // 2
+    member = routes[None, :, :] == jnp.arange(experts, dtype=jnp.int32)[:, None, None]
+    dense = jnp.sum(jnp.where(member, route_weights[None, :, :], 0.0), axis=2)
+    gain = norm_gain[None, :]
+    outputs = whole(
+        tokens, dense.reshape(experts, 2, 1, share), gain,
+        (shared_gate, shared_up, shared_down), (expert_gate, expert_up, expert_down),
+    )
+    (
+        layer_output, sample_gate, sample_up, sample_down, common_gate, common_up, common_down
+    ) = emit(*outputs)
+    return (
+        layer_output, sample_gate[None], sample_up[None], sample_down[None],
+        common_gate, common_up, common_down,
+    )
+
 
 def solution(mesh):
+    fits = mesh.shape["fs"] == 16 and mesh.shape["tp"] == 2
+    body = block_body if fits else general_body
     return jax.shard_map(
         body,
         mesh=mesh,

time: 482 us -> 320 us (0.66)
  Pallas kernels: 0 us -> 314 us
  waiting for transfers between devices: 209 us -> 0 us
  blocking collectives: 124 us -> 0 us
  matrix products: 57.7 us -> 0 us
  local copies, waits for them, and re-layouts: 37.6 us -> 0.62 us
  starting transfers between devices: 19.7 us -> 0 us
  other arithmetic: 17.1 us -> 0.73 us
  between operations: 14.1 us -> 0.64 us
    pallas_call x0 -> x2, Pallas kernels: none -> 314 us  [the longest x1 304 us: whole(): pl.pallas_call(whole_kernel, out_shape=[jax.ShapeDtypeStruct((tok_rows, w...]
    all_to_all x2 -> x0, waiting for transfers between devices: 143 us -> none  [the longest x1 84.8 us: body(): lax.all_to_all(rounded[1], 'fs', split_axis=0, concat_axis=1, tiled=True)]
    all_to_all x3 -> x0, blocking collectives: 96.5 us -> none  [the longest x1 87.8 us: body(): lax.all_to_all(rounded[0], 'fs', split_axis=0, concat_axis=1, tiled=True)]
    reduce_scatter x1 -> x0, waiting for transfers between devices: 66 us -> none  [body(): lax.psum_scatter(total.astype(jnp.bfloat16), 'fs', scatter_dimension=0, t...]
    dot_general x7 -> x0, matrix products: 57.7 us -> none  [the longest x2 30.2 us: body(): jnp.einsum('rf,df->rd', hidden, down_w, preferred_element_type=jnp.float32)]
    unnamed x63 -> x0, local copies, waits for them, and re-layouts: 32.5 us -> none
    all_gather x1 -> x0, blocking collectives: 28 us -> none  [body(): dense_all = lax.all_gather(dense, 'fs', axis=0, tiled=False)]
    convert_element_type x6 -> x0, other arithmetic: 14.6 us -> none  [the longest x1 6.12 us: body(): (expert_up * gain_rows).astype(jnp.bfloat16)]
  transfers between devices with their start and end apart: 8 -> 0, of which waited for: 3 -> 0; matrix products, arithmetic and copies ran while one was open for 20% -> 0% of each run, Pallas kernels for 0% -> 0%
where the time goes in v3:
time: 320 us; the launch traced here: 316 us
  Pallas kernels  314 us (98%)
    pallas_call x1, Pallas kernels, whole(): pl.pallas_call(whole_kernel, out_shape=[jax.ShapeDtypeStruct((tok_rows, w...  304 us
    pallas_call x1, Pallas kernels, emit(): pl.pallas_call(functools.partial(emit_kernel, n), out_shape=shapes, in_sp...  10.1 us

profile of v3, /device:TPU:9, one launch (start us, length us, event | category | flops | bytes accessed | tf_op | source)
XLA Modules:
  0.0 315.8 jit_solution(7901888148287259823)
XLA Ops:
  0.6 0.7 select_reduce_fusion
  1.4 0.6 reshape.19.scale_ref
  2.0 303.7 %whole.1 = (bf16[256,1024]{1,0:T(8,128)(2,1)}, bf16[2048,512]{1,0:T(8,128)(2,1)}, bf16[2048,512]{1,0:T(8,128)(2,1)}, bf16[2048,512]{1,0:T(8,128)(2,1)}, bf16[204...) custom-call(bf16[256,2048]{1,0:T(8,128)(2,1)} %tok_ref.1, ...), custom_call_target="tpu_custom_call" | custom-call | tf_op jit(solution)/shard_map/whole/pallas_call | solution.py:567
  305.7 10.1 %emit.1 = (bf16[256,1024]{1,0:T(8,128)(2,1)}, bf16[2048,512]{1,0:T(8,128)(2,1)}, bf16[2048,512]{1,0:T(8,128)(2,1)}, bf16[2048,512]{1,0:T(8,128)(2,1)}, bf16[2048...) custom-call(bf16[256,1024]{1,0:T(8,128)(2,1)} %get-tuple-element.21.refs_0_, ...), custom_call_target="tpu_custom_call" | custom-call | tf_op jit(solution)/shard_map/emit/pallas_call | solution.py:631

commit v4 on v3

--- a/solution.py
+++ b/solution.py
@@ -23,7 +23,7 @@
     return fs, lax.axis_index("tp"), fs % 2, (fs // 2) % 2, fs // 4
 
 
-def barrier_all(fs, tp):
+def greet(fs, tp):
     count = lax.axis_size("fs")
     sem = pltpu.get_barrier_semaphore()
     for step in range(1, count):
@@ -31,7 +31,10 @@
             sem, inc=1, device_id=((fs + step) % count, tp), device_id_type=MESH
         )
     pl.semaphore_signal(sem, inc=1, device_id=(fs, 1 - tp), device_id_type=MESH)
-    pl.semaphore_wait(sem, count)
+
+
+def meet():
+    pl.semaphore_wait(pltpu.get_barrier_semaphore(), lax.axis_size("fs"))
 
 
 def column(row):
@@ -100,6 +103,12 @@
         z = self.z
         pl.when(z - step - 1 >= 0)(lambda: self.arrive(z - step - 1, kinds))
         pl.when(z + step + 1 < 4)(lambda: self.arrive(z + step + 1, kinds))
+
+    def fan(self, step):
+        z = self.z
+        pl.when(z - step >= 0)(lambda: self.spread(z - step, (2, 3)))
+        if step > 0:
+            pl.when(z + step < 4)(lambda: self.spread(z + step, (2, 3)))
 
     def turn(self, step):
         self.plane_forward(self.z - step)
@@ -231,10 +240,10 @@
     tok_ref, scale_ref, gain_ref, sgate_ref, sup_ref, sdown_ref, gate_ref, up_ref, down_ref,
     out_ref, sample_gate, sample_up, sample_down, common_gate, common_up, common_down,
     acts, gate_up, down_v, wide, narrow, hidden, common, normed, scales, scol,
-    shid, spart, spart_in, fin, fin_in, xd_in, yd_in, xg_in, yg_in, zb_in, za_in,
+    shid, spart, spart_in, fin, fin_in, xd_in, yd_in, xg_in, yg_in, zb_in, za_in, lb_in, la_in,
     t_send, t_fwd, t_recv, c_send, c_fwd, c_recv, sc_send, sc_recv,
     load_sem, w_send, w_recv, p_send, p_recv,
-    d_send, d_recv, g_send, g_recv, z_send, z_recv, e_send, e_recv, loc_sem,
+    d_send, d_recv, g_send, g_recv, z_send, z_recv, l_send, l_recv, e_send, e_recv, loc_sem,
 ):
     fs, tp, x, y, z = place()
     rows, half = sgate_ref.shape
@@ -251,22 +260,25 @@
     )
     chain = Chain(lambda slot: common.at[pl.ds(slot * rows, rows)], c_send, c_fwd, c_recv)
 
+    greet(fs, tp)
+    own_tokens = pltpu.make_async_copy(tok_ref, normed, loc_sem.at[7])
+    own_tokens.start()
     ex.each(1, 17, lambda to: ex.load(0, to).start())
+    own_tokens.wait()
+    normed[...] = normalize(normed[...])
+    acts[z, pl.ds((fs % 4) * share, share), :] = normed[
+        pl.ds(pl.multiple_of(tp * share, share), share), :
+    ]
     gain = column(gain_ref[...])
     mine = pl.ds(fs * rows, rows)
     common[mine, 0:half] = (sgate_ref[...] * gain).astype(jnp.bfloat16)
     common[mine, half : 2 * half] = (sup_ref[...] * gain).astype(jnp.bfloat16)
     common[mine, 2 * half : 3 * half] = sdown_ref[...].astype(jnp.bfloat16)
-    normed[...] = normalize(tok_ref[...])
-    acts[z, pl.ds((fs % 4) * share, share), :] = normed[
-        pl.ds(pl.multiple_of(tp * share, share), share), :
-    ]
+    meet()
+
+    tokens.spread(z)
     ex.convert(0, gain)
     ex.convert(1, gain)
-    ex.convert(2, None)
-    barrier_all(fs, tp)
-
-    tokens.spread(z)
 
     def scale_copy(to):
         return remote(
@@ -277,6 +289,7 @@
     own_scale.start()
     ex.each(1, 16, lambda to: scale_copy(to).start())
     ex.send(1, 5, (0, 1))
+    ex.convert(2, None)
     tokens.hop(0)
     tokens.turn(0)
     ex.send(5, 6, (0, 1))
@@ -293,10 +306,11 @@
     ex.send(12, 16, (0, 1))
     ex.send(4, 16, (2,))
     tokens.turn(3)
+    for step in range(3):
+        chain.fan(step)
     chain.hop(2, along)
+    chain.fan(3)
     ex.send(1, 4, (2,))
-    for block in range(4):
-        chain.spread(block, (2, 3))
     ex.keep((0, 1, 2))
     own_scale.wait()
 
@@ -350,29 +364,43 @@
     plane = fs % 4
     xp, yp = chain.xp, chain.yp
     xplane, yplane, dplane = chain.xplane, chain.yplane, 3 - plane
-    mid, quarter = width // 2, width // 4
+    mid, quarter = 3 * width // 8, 3 * width // 16
+    tail, eighth = width // 4, width // 8
+    last = pl.ds(2 * mid, tail)
+    mixed = 2
 
     def columns(side):
+        if side == mixed:
+            return pl.ds(2 * mid, eighth), pl.ds(2 * mid + eighth, eighth)
         return pl.ds(side * mid, quarter), pl.ds(side * mid + quarter, quarter)
+
+    def box_of(side):
+        if side == mixed:
+            return pl.ds(2 * quarter, eighth)
+        return pl.ds(side * quarter, quarter)
+
+    def number(b, side):
+        return 8 if side == mixed else 2 * b + side
 
     def part(b, which, cols):
         return acts.at[b, pl.ds(which * share, share), cols]
 
     def down_unit(b, side):
+        start = side * mid
+
         def step(n, carry):
-            cols = pl.ds(pl.multiple_of(side * mid + n * tile, tile), tile)
+            cols = pl.ds(pl.multiple_of(start + n * tile, tile), tile)
             acts[b, :, cols] = (
                 dot_nt(hidden[b, :, 0:half], down_v[0, cols, :])
                 + dot_nt(hidden[b, :, half : 2 * half], down_v[1, cols, :])
             ).astype(jnp.bfloat16)
             return carry
 
-        lax.fori_loop(0, mid // tile, step, 0)
+        lax.fori_loop(0, (tail if side == mixed else mid) // tile, step, 0)
 
     def d_copies(b, side):
         lo, hi = columns(side)
-        box = pl.ds(side * quarter, quarter)
-        n = 2 * b + side
+        box, n = box_of(side), number(b, side)
         return (
             remote(
                 part(b, dplane, lo), xd_in.at[b, :, box], d_send.at[0, n], d_recv.at[0, n], xp, tp
@@ -390,7 +418,7 @@
             (yplane, hi, yg_in, yp),
             (yplane, lo, yg_in, yp),
         )[kind]
-        n = 2 * b + side
+        n = number(b, side)
         return remote(
             part(b, which, cols), box.at[b, :, cols], g_send.at[kind, n], g_recv.at[kind, n],
             to, tp,
@@ -410,7 +438,7 @@
 
     def combine(b, side):
         lo, hi = columns(side)
-        box = pl.ds(side * quarter, quarter)
+        box = box_of(side)
         x_copy, y_copy = d_copies(b, side)
         x_copy.wait_recv()
         add_into(part(b, yplane, lo), [xd_in.at[b, :, box]])
@@ -419,54 +447,98 @@
         add_into(part(b, xplane, hi), [yd_in.at[b, :, box]])
         g_copy(b, side, 1).start()
 
+    def z_box(b, way, cols):
+        return (zb_in.at[max(b - 1, 0), :, cols], za_in.at[min(b, 2), :, cols])[way]
+
     def z_copy(b, side, way):
-        box = (zb_in, za_in)[way]
         cols = pl.ds(side * mid, mid)
         n = 2 * b + side
         return remote(
-            part(b, plane, cols), box.at[b, :, cols], z_send.at[way, n], z_recv.at[way, n],
+            part(b, plane, cols), z_box(b, way, cols), z_send.at[way, n], z_recv.at[way, n],
             fs + (4, -4)[way], tp,
         )
 
     def settle(b, side):
-        cols = pl.ds(side * mid, mid)
+        cols = last if side == mixed else pl.ds(side * mid, mid)
         for kind in range(4):
             g_copy(b, side, kind).wait_recv()
         add_into(part(b, plane, cols), [xg_in.at[b, :, cols], yg_in.at[b, :, cols]])
+        if side == mixed:
+            return
         if b > 0:
             pl.when(z == 0)(z_copy(b, side, 0).start)
         if b < 3:
             pl.when(z == 3)(z_copy(b, side, 1).start)
 
-    def relay(b, side):
+    def relay(b, side, second):
         cols = pl.ds(side * mid, mid)
-        if b > 0:
-            @pl.when(jnp.logical_and(z > 0, z < b))
-            def _():
-                z_copy(b, side, 0).wait_recv()
-                add_into(part(b, plane, cols), [zb_in.at[b, :, cols]])
-                z_copy(b, side, 0).start()
-
-        if b < 3:
-            @pl.when(jnp.logical_and(z < 3, z > b))
-            def _():
-                z_copy(b, side, 1).wait_recv()
-                add_into(part(b, plane, cols), [za_in.at[b, :, cols]])
-                z_copy(b, side, 1).start()
+        for at, way in ((1, 0), (2, 0), (1, 1), (2, 1)):
+            if (at >= b if way == 0 else at <= b):
+                continue
+            if second != ((way, at) in ((0, 2), (1, 1))):
+                continue
+
+            @pl.when(z == at)
+            def _(way=way):
+                z_copy(b, side, way).wait_recv()
+                add_into(part(b, plane, cols), [z_box(b, way, cols)])
+                z_copy(b, side, way).start()
 
     def finish(b):
         @pl.when(z == b)
         def _():
             for side in range(2):
-                cols = pl.ds(side * mid, mid)
+                if b > 0:
+                    z_copy(b, side, 0).wait_recv()
+                if b < 3:
+                    z_copy(b, side, 1).wait_recv()
+            for side, lower, upper in ((0, 0, width // 2), (1, width // 2, 2 * mid)):
+                cols = pl.ds(lower, upper - lower)
                 total = acts[b, pl.ds(plane * share, share), cols].astype(jnp.float32)
                 if b > 0:
-                    z_copy(b, side, 0).wait_recv()
-                    total = total + zb_in[b, :, cols].astype(jnp.float32)
+                    total = total + z_box(b, 0, cols)[...].astype(jnp.float32)
                 if b < 3:
-                    z_copy(b, side, 1).wait_recv()
-                    total = total + za_in[b, :, cols].astype(jnp.float32)
-                fin[side] = total.astype(jnp.bfloat16)
+                    total = total + z_box(b, 1, cols)[...].astype(jnp.float32)
+                fin[side, :, 0 : upper - lower] = total.astype(jnp.bfloat16)
+            fin[1, :, 2 * mid - width // 2 : width // 2] = acts[
+                b, pl.ds(plane * share, share), last
+            ]
+
+    def l_box(b, way):
+        return (lb_in.at[max(b - 1, 0)], la_in.at[min(b, 2)])[way]
+
+    def line_copy(b, way):
+        return remote(
+            acts.at[b, :, last], l_box(b, way), l_send.at[way, b], l_recv.at[way, b],
+            fs + (4, -4)[way], tp,
+        )
+
+    def line_start():
+        for b in (3, 2, 1):
+            pl.when(z == 0)(line_copy(b, 0).start)
+        for b in (0, 1, 2):
+            pl.when(z == 3)(line_copy(b, 1).start)
+
+    def line_relay(b, at):
+        way = 0 if at < b else 1
+
+        @pl.when(z == at)
+        def _():
+            line_copy(b, way).wait_recv()
+            add_into(acts.at[b, :, last], [l_box(b, way)])
+            line_copy(b, way).start()
+
+    def line_end(b):
+        @pl.when(z == b)
+        def _():
+            boxes = []
+            if b > 0:
+                line_copy(b, 0).wait_recv()
+                boxes.append(l_box(b, 0))
+            if b < 3:
+                line_copy(b, 1).wait_recv()
+                boxes.append(l_box(b, 1))
+            add_into(acts.at[b, :, last], boxes)
 
     puts = [
         pltpu.make_async_copy(common.at[:, pl.ds(i * half, half)], ref, loc_sem.at[4 + i])
@@ -485,7 +557,7 @@
         return carry
 
     def shared_down_step(n, carry):
-        per = mid // tile
+        per = width // 2 // tile
         spart[n // per, :, pl.ds(pl.multiple_of((n % per) * tile, tile), tile)] = dot_nt(
             shid[...],
             common[pl.ds(pl.multiple_of(n * tile, tile), tile), 2 * half : 3 * half],
@@ -504,22 +576,45 @@
 
     pieces = [(b, side) for b in UNITS for side in range(2)]
     count = len(pieces)
-    for i in range(count + 4):
+    for i in range(count + 6):
         if i < count:
             down_unit(*pieces[i])
             first(*pieces[i])
+        if i == 0:
+            for b in UNITS:
+                down_unit(b, mixed)
+            line_start()
         if i == 1:
             chain.plane_forward(2)
         if i == 2:
             chain.plane_forward(3)
-        if i == count + 1:
+        if i == 5:
             shared_expert()
         if 1 <= i <= count:
             combine(*pieces[i - 1])
         if 2 <= i <= count + 1:
             settle(*pieces[i - 2])
-        if i >= 4:
-            relay(*pieces[i - 4])
+        if i == 2:
+            line_relay(0, 2)
+            line_relay(3, 1)
+        if i == 3:
+            line_relay(1, 2)
+            line_relay(2, 1)
+        if i == 4:
+            line_relay(0, 1)
+            line_relay(3, 2)
+        if i == 6:
+            for b in range(4):
+                line_end(b)
+            first(z, mixed)
+        if i == 7:
+            combine(z, mixed)
+        if i == count + 1:
+            settle(z, mixed)
+        if 4 <= i < count + 4:
+            relay(*pieces[i - 4], False)
+        if i >= 6:
+            relay(*pieces[i - 6], True)
     for b in UNITS:
         finish(b)
     f_copy = remote(fin.at[1 - tp], fin_in, e_send.at[1], e_recv.at[1], fs, 1 - tp)
@@ -542,11 +637,18 @@
         copy.wait()
     chain.drain()
     ex.drain()
-    for b, side in pieces:
+    for b in range(4):
+        if b > 0:
+            pl.when(z < b)(line_copy(b, 0).wait_send)
+        if b < 3:
+            pl.when(z > b)(line_copy(b, 1).wait_send)
+    for b, side in pieces + [(z, mixed)]:
         for copy in d_copies(b, side):
             copy.wait_send()
         for kind in range(4):
             g_copy(b, side, kind).wait_send()
+        if side == mixed:
+            continue
         if b > 0:
             pl.when(z < b)(z_copy(b, side, 0).wait_send)
         if b < 3:
@@ -567,7 +669,7 @@
     return pl.pallas_call(
         whole_kernel,
         out_shape=[jax.ShapeDtypeStruct((tok_rows, width // 2), bf16)] + [weight] * 6,
-        in_specs=[VMEM] * 6 + [HBM] * 3,
+        in_specs=[HBM] + [VMEM] * 5 + [HBM] * 3,
         out_specs=[VMEM] + [HBM] * 6,
         scratch_shapes=[
             pltpu.VMEM((4, 4 * share, width), bf16),
@@ -589,12 +691,15 @@
             pltpu.VMEM((4, share, width // 2), bf16),
             pltpu.VMEM((4, share, width), bf16),
             pltpu.VMEM((4, share, width), bf16),
-            pltpu.VMEM((4, share, width), bf16),
-            pltpu.VMEM((4, share, width), bf16),
+            pltpu.VMEM((3, share, 3 * width // 4), bf16),
+            pltpu.VMEM((3, share, 3 * width // 4), bf16),
+            pltpu.VMEM((3, 4 * share, width // 4), bf16),
+            pltpu.VMEM((3, 4 * share, width // 4), bf16),
             DMA((4, 4)), DMA((4,)), DMA((16,)), DMA((4, 4)), DMA((4,)), DMA((16,)),
             DMA((16,)), DMA((16,)),
             DMA((3, 16)), DMA((3, 16)), DMA((3, 16)), DMA((3, 16)), DMA((3, 16)),
-            DMA((2, 8)), DMA((2, 8)), DMA((4, 8)), DMA((4, 8)), DMA((2, 8)), DMA((2, 8)),
+            DMA((2, 9)), DMA((2, 9)), DMA((4, 9)), DMA((4, 9)), DMA((2, 8)), DMA((2, 8)),
+            DMA((2, 4)), DMA((2, 4)),
             DMA((2,)), DMA((2,)), DMA((8,)),
         ],
         compiler_params=pltpu.CompilerParams(

time: 320 us -> 304 us (0.950)
  Pallas kernels: 314 us -> 300 us
    pallas_call x1, Pallas kernels: 304 us -> 290 us  [whole(): pl.pallas_call(whole_kernel, out_shape=[jax.ShapeDtypeStruct((tok_rows, w...]
where the time goes in v4:
time: 304 us; the launch traced here: 302 us
  Pallas kernels  300 us (99%)
    pallas_call x1, Pallas kernels, whole(): pl.pallas_call(whole_kernel, out_shape=[jax.ShapeDtypeStruct((tok_rows, w...  290 us
    pallas_call x1, Pallas kernels, emit(): pl.pallas_call(functools.partial(emit_kernel, n), out_shape=shapes, in_sp...  10.1 us

profile of v4, /device:TPU:9, one launch (start us, length us, event | category | flops | bytes accessed | tf_op | source)
XLA Modules:
  0.0 302.3 jit_solution(16707524110491254399)
XLA Ops:
  0.6 0.7 select_reduce_fusion
  1.4 0.6 reshape.19.scale_ref
  2.0 290.1 %whole.1 = (bf16[256,1024]{1,0:T(8,128)(2,1)}, bf16[2048,512]{1,0:T(8,128)(2,1)}, bf16[2048,512]{1,0:T(8,128)(2,1)}, bf16[2048,512]{1,0:T(8,128)(2,1)}, bf16[204...) custom-call(bf16[256,2048]{1,0:T(8,128)(2,1)} %tok_ref.1, ...), custom_call_target="tpu_custom_call" | custom-call | tf_op jit(solution)/shard_map/whole/pallas_call | solution.py:669
  292.1 10.1 %emit.1 = (bf16[256,1024]{1,0:T(8,128)(2,1)}, bf16[2048,512]{1,0:T(8,128)(2,1)}, bf16[2048,512]{1,0:T(8,128)(2,1)}, bf16[2048,512]{1,0:T(8,128)(2,1)}, bf16[2048...) custom-call(bf16[256,1024]{1,0:T(8,128)(2,1)} %get-tuple-element.21.refs_0_, ...), custom_call_target="tpu_custom_call" | custom-call | tf_op jit(solution)/shard_map/emit/pallas_call | solution.py:736
